TPU v7x, 32 devices: a whole 2x2x4 slice. The times are simulated.
32 devices in a mesh: sp: 16 (over z, y, x), tp: 2 (over core).
Axes of the slice: x: 2, y: 2, z: 4, core: 2. Of those that a mesh axis runs over, the one named last changes fastest.
Arguments:
- tokens: bfloat16 [6144, 2048], P('sp', 'tp'), may hold values from -6 to 6
- input_gain: float32 [2048], replicated, may hold values from 0.1 to 1.9
- query_weight: bfloat16 [2048, 1024], P(None, 'tp'), may hold values from -0.5 to 0.5
- query_rot_weight: bfloat16 [2048, 512], P(None, 'tp'), may hold values from -0.125 to 0.125
- kv_down: bfloat16 [2048, 256], replicated, may hold values from -0.5 to 0.5
- rot_down: bfloat16 [2048, 32], replicated, may hold values from -0.125 to 0.125
- kv_gain: float32 [256], replicated, may hold values from 0.1 to 1.9
- key_up: bfloat16 [256, 1024], P(None, 'tp'), may hold values from -0.5 to 0.5
- value_up: bfloat16 [256, 1024], P(None, 'tp'), may hold values from -4 to 4
- conv_value_weight: bfloat16 [2048, 1024], P(None, 'tp'), may hold values from -0.125 to 0.125
- conv_gate_weight: bfloat16 [2048, 1024], P(None, 'tp'), may hold values from -0.125 to 0.125
- conv_taps: float32 [31, 1024], P(None, 'tp'), may hold values from -8 to 8
- conv_ln_gain: float32 [1024], P('tp'), may hold values from 0.1 to 1.9
- conv_ln_bias: float32 [1024], P('tp'), may hold values from -3 to 3
- att_out_gain: float32 [1024], P('tp'), may hold values from 0.1 to 1.9
- conv_out_gain: float32 [1024], P('tp'), may hold values from 0.1 to 1.9
- att_out_weight: bfloat16 [1024, 2048], P('tp'), may hold values from -0.125 to 0.125
- conv_out_weight: bfloat16 [1024, 2048], P('tp'), may hold values from -0.125 to 0.125
Outputs:
- mixed: bfloat16 [6144, 2048], P('sp', 'tp')
All inputs are finite; a program needn't handle non-finite values.
Results may differ from a plain program's by a relative error of at most 0.017.
Values may be sent and summed in bfloat16 or wider, within the bound.
No kernel may reach another device: no remote copies, remote signals or barrier semaphores. Data moves between devices by JAX's collectives and lax.ppermute only.
A program may use at most 128 MiB of HBM per device.

v0:
```python
import functools
import math

import jax
import jax.numpy as jnp
from jax import lax
from jax.experimental import pallas as pl
from jax.experimental.pallas import tpu as pltpu
from jax.sharding import PartitionSpec as P


D_MODEL = 2048
NOPE_DIM = 64
ROT_DIM = 32
VALUE_DIM = 64
CONV_CH = 1024
KERNEL = 31
ATT_WIDTH = 1024


norm_eps = 1e-06
far_below = -1e30
rope_base = 10000.0
SUM_ROWS = 16


def rotary_tables(positions, half_dim):
    frequency = rope_base ** (-jnp.arange(half_dim, dtype=jnp.float32) / half_dim)
    angles = positions.astype(jnp.float32)[:, None] * frequency[None, :]
    return (jnp.cos(angles), jnp.sin(angles))


def rotate_half(values, cos_table, sine_table):
    half_dim = cos_table.shape[-1]
    front_half = values[..., :half_dim]
    back_half = values[..., half_dim:]
    return jnp.concatenate(
        [
            front_half * cos_table - back_half * sine_table,
            back_half * cos_table + front_half * sine_table,
        ],
        axis=-1,
    )


def shift_by(block, axis, distance):
    devices = range(lax.axis_size(axis))
    return lax.ppermute(block, axis, [(i, i + distance) for i in devices if i + distance in devices])


def swap_bits(block, axis, bits):
    return lax.ppermute(block, axis, [(i, i ^ bits) for i in range(lax.axis_size(axis))])


def others(block, axis):
    size = lax.axis_size(axis)
    return [
        lax.ppermute(block, axis, [((i + d) % size, i) for i in range(size)])
        for d in range(1, size)
    ]


def total(block, axis):
    for part in others(block, axis):
        block = block + part
    return block


def front_kernel(pieces, rows, groups, index_ref, *refs):
    token_refs, refs = refs[:pieces], refs[pieces:]
    gain_ref, down_ref, rot_down_ref, kv_gain_ref, cos_ref, sin_ref = refs[:6]
    scaled_ref, scale_ref, lat_ref, rot_ref, send_ref, wide_rot_ref = refs[6:]
    me = index_ref[0]
    tok_rows, width = token_refs[0].shape
    squares = jnp.zeros((tok_rows, 128), jnp.float32)
    for d, ref in enumerate(token_refs):
        begin = lax.rem(me + d, pieces) * width
        for col in range(0, width, 128):
            at = pl.ds(pl.multiple_of(begin + col, 128), 128)
            values = ref[:, col : col + 128].astype(jnp.float32)
            scaled_ref[:, at] = (values * gain_ref[:, at]).astype(jnp.bfloat16)
            squares = squares + values * values
    row_scale = lax.rsqrt(jnp.sum(squares, axis=1, keepdims=True) / D_MODEL + norm_eps)
    scale_ref[...] = row_scale
    raw = jnp.dot(scaled_ref[...], down_ref[...], preferred_element_type=jnp.float32)
    half = ROT_DIM // 2
    turned = jnp.concatenate(
        [rot_down_ref[...], rot_down_ref[half:, :], rot_down_ref[:half, :]], axis=0
    )
    both = (
        lax.dot_general(
            scaled_ref[...], turned, (((1,), (1,)), ((), ())), preferred_element_type=jnp.float32
        )
        * row_scale
    )
    mean = jnp.mean(raw * raw, axis=1, keepdims=True)
    lat_ref[...] = (raw * lax.rsqrt(mean + norm_eps) * kv_gain_ref[...]).astype(jnp.bfloat16)
    rot = both[:, :ROT_DIM] * cos_ref[...] + both[:, ROT_DIM : 2 * ROT_DIM] * sin_ref[...]
    rot = jnp.concatenate([rot, jnp.zeros((tok_rows, 128 - ROT_DIM), jnp.float32)], axis=1)
    wide_rot_ref[...] = rot
    rot_ref[...] = rot.astype(jnp.bfloat16)
    start = me * rows
    send_ref[:rows, :] = lat_ref[pl.ds(pl.multiple_of(start, 16), rows), :]
    height = rows // groups
    packed = [
        wide_rot_ref[pl.ds(pl.multiple_of(start + g * height, 8), height), :][:, :ROT_DIM]
        for g in range(groups)
    ]
    rank = lat_ref.shape[1]
    if groups * ROT_DIM < rank:
        packed.append(jnp.zeros((height, rank - groups * ROT_DIM), jnp.float32))
    packed = jnp.concatenate(packed, axis=1)
    spare = send_ref.shape[0] - rows - height
    if spare:
        packed = jnp.concatenate([packed, jnp.zeros((spare, rank), jnp.float32)], axis=0)
    send_ref[rows:, :] = packed.astype(jnp.bfloat16)


def front(index, pieces, gain, down, rot_down, kv_gain, cos, sin, groups):
    tok_rows, width = pieces[0].shape
    rank = down.shape[1]
    rows = tok_rows // len(pieces)
    height = rows // groups
    model = width * len(pieces)
    in_vmem = pl.BlockSpec()
    args = list(pieces) + [gain, down, rot_down, kv_gain, cos, sin]
    return pl.pallas_call(
        functools.partial(front_kernel, len(pieces), rows, groups),
        in_specs=[pl.BlockSpec(memory_space=pltpu.SMEM)] + [in_vmem] * len(args),
        out_specs=(in_vmem,) * 5,
        out_shape=(
            jax.ShapeDtypeStruct((tok_rows, model), jnp.bfloat16),
            jax.ShapeDtypeStruct((tok_rows, 1), jnp.float32),
            jax.ShapeDtypeStruct((tok_rows, rank), jnp.bfloat16),
            jax.ShapeDtypeStruct((tok_rows, 128), jnp.bfloat16),
            jax.ShapeDtypeStruct((rows + height + -height % 16, rank), jnp.bfloat16),
        ),
        scratch_shapes=[pltpu.VMEM((tok_rows, 128), jnp.float32)],
        compiler_params=pltpu.CompilerParams(vmem_limit_bytes=16 * 1024 * 1024),
        cost_estimate=pl.CostEstimate(
            flops=2 * tok_rows * model * 512, bytes_accessed=8 << 20, transcendentals=tok_rows
        ),
        name="front",
    )(index, *args)


def tiles_of(queries):
    width = 256 if (2 * queries) % 256 == 0 else queries
    out = []
    for start in range(0, 2 * queries, width):
        parts = []
        for side in range(2):
            low = max(start, side * queries)
            high = min(start + width, (side + 1) * queries)
            if low < high:
                parts.append((side, low - start, high - start))
        out.append((start, parts))
    return width, out


def attention_kernel(first, last, counts, rows, groups, heads, vis_ref, *refs):
    refs = list(refs)
    qt_ref, qrt_ref, key_up_ref, value_up_ref = refs[:4]
    refs = refs[4:]
    pieces = len(counts[0])
    sources = []
    for _ in counts:
        sources.append(refs[:pieces])
        refs = refs[pieces:]
    if first:
        (own_lat_ref, own_rot_ref), refs = refs[:2], refs[2:]
    else:
        (max_in, acc_in), refs = refs[:2], refs[2:]
    if last:
        (out_ref, max_ref, acc_ref), refs = refs[:3], refs[3:]
    else:
        (max_ref, acc_ref), refs = refs[:2], refs[2:]
    lat_ref, rot_ref, qbd_ref, turned_ref, score_refs, weight_refs, refs = (
        refs[0], refs[1], refs[2], refs[3], refs[4:6], refs[6:8], refs[8:]
    )
    pairs = heads // 2
    parcels = max(1, pairs // 2)
    key_refs, values_refs = refs[:parcels], refs[parcels:]
    per = pairs // parcels
    queries = qt_ref.shape[1]
    width, tiles = tiles_of(queries)
    head_rows = VALUE_DIM + SUM_ROWS
    blocks = lat_ref.shape[0]
    bias_row = 2 * NOPE_DIM + ROT_DIM

    turned_ref[...] = value_up_ref[...].T
    qbd_ref[...] = jnp.zeros_like(qbd_ref)
    for pair in range(pairs):
        qbd_ref[pair, bias_row : bias_row + 16, :] = (
            lax.broadcasted_iota(jnp.int32, (16, 2 * queries), 0) == 0
        ).astype(jnp.bfloat16)
        for side in range(2):
            head = 2 * pair + side
            columns = slice(side * queries, (side + 1) * queries)
            qbd_ref[pair, side * NOPE_DIM : (side + 1) * NOPE_DIM, columns] = qt_ref[
                head * NOPE_DIM : (head + 1) * NOPE_DIM, :
            ]
            qbd_ref[pair, 2 * NOPE_DIM : 2 * NOPE_DIM + ROT_DIM, columns] = qrt_ref[
                head * ROT_DIM : (head + 1) * ROT_DIM, :
            ]
    for ref in values_refs:
        ref[...] = jnp.ones_like(ref)
    if first:
        max_ref[...] = jnp.full_like(max_ref, far_below)
        acc_ref[...] = jnp.zeros_like(acc_ref)
        lat_ref[0, :queries, :] = own_lat_ref[...]
        rot_ref[0, :queries, :] = own_rot_ref[...]
    else:
        max_ref[...] = max_in[...]
        acc_ref[...] = acc_in[...]

    at = 1 if first else 0
    slot = 0
    is_bias = lax.broadcasted_iota(jnp.int32, (queries, 128), 1) == ROT_DIM
    for source, several in zip(sources, counts):
        for index in range(several[0] or 1):
            rots = []
            base = (at % 2) * queries
            for n, ref in enumerate(source):
                view = ref.at[index] if several[0] else ref
                lat_ref[at // 2, base + n * rows : base + (n + 1) * rows, :] = view[:rows, :]
                packed = view[rows:, :].astype(jnp.float32)[: rows // groups]
                rots += [packed[:, g * ROT_DIM : (g + 1) * ROT_DIM] for g in range(groups)]
            rot = jnp.concatenate(rots, axis=0)
            rot = jnp.concatenate([rot, jnp.zeros((queries, 128 - ROT_DIM), jnp.float32)], axis=1)
            bias = jnp.where(vis_ref[slot] > 0, 0.0, far_below)
            rot_ref[at // 2, base : base + queries, :] = jnp.where(is_bias, bias, rot).astype(jnp.bfloat16)
            at += 1
            slot += 1
    if at % 2:
        lat_ref[at // 2, queries:, :] = jnp.zeros((queries, lat_ref.shape[2]), jnp.bfloat16)
        rot_ref[at // 2, queries:, :] = jnp.where(is_bias, far_below, 0.0).astype(jnp.bfloat16)

    def visit(block, masked):
        span = per * 2 * NOPE_DIM
        work = [(pair, i) for pair in range(pairs) for i in range(len(tiles))]
        shrinks = {}

        def expand_keys(n):
            key_refs[n][...] = jnp.dot(
                lat_ref[block],
                key_up_ref[:, n * span : (n + 1) * span],
                preferred_element_type=jnp.float32,
            ).astype(jnp.bfloat16)

        def expand_values(n):
            values = lax.dot_general(
                turned_ref[n * span : (n + 1) * span, :],
                lat_ref[block],
                (((1,), (1,)), ((), ())),
                preferred_element_type=jnp.float32,
            ).astype(jnp.bfloat16)
            for head in range(2 * per):
                values_refs[n][head * head_rows : head * head_rows + VALUE_DIM, :] = values[
                    head * VALUE_DIM : (head + 1) * VALUE_DIM, :
                ]

        def product(at):
            pair, i = work[at]
            begin = tiles[i][0]
            within = (pair % per) * 2 * NOPE_DIM
            key_pair = jnp.concatenate(
                [key_refs[pair // per][:, within : within + 2 * NOPE_DIM], rot_ref[block]], axis=1
            )
            score = jnp.dot(
                key_pair, qbd_ref[pair, :, begin : begin + width], preferred_element_type=jnp.float32
            )
            if masked:
                column = lax.broadcasted_iota(jnp.int32, (queries, width), 1) + begin
                column = jnp.where(column >= queries, column - queries, column)
                visible = lax.broadcasted_iota(jnp.int32, (queries, width), 0) <= column
                score_refs[at % 2][:queries, :] = jnp.where(visible, score[:queries], far_below)
                score_refs[at % 2][queries:, :] = score[queries:]
            else:
                score_refs[at % 2][...] = score

        def soften(at):
            old_max = max_ref[at : at + 1, :]
            score = score_refs[at % 2]
            new_max = jnp.maximum(old_max, jnp.max(score[...], axis=0, keepdims=True))
            weight_refs[at % 2][...] = jnp.exp2(score[...] - new_max).astype(jnp.bfloat16)
            shrinks[at] = jnp.exp2(old_max - new_max)
            max_ref[at : at + 1, :] = new_max

        def weigh(at):
            pair, i = work[at]
            parts = tiles[i][1]
            head = 2 * (pair % per) + parts[0][0]
            fresh = jnp.dot(
                values_refs[pair // per][head * head_rows : (head + len(parts)) * head_rows, :],
                weight_refs[at % 2][...],
                preferred_element_type=jnp.float32,
            )
            if len(parts) > 1:
                fresh = jnp.concatenate(
                    [
                        fresh[n * head_rows : (n + 1) * head_rows, low:high]
                        for n, (_, low, high) in enumerate(parts)
                    ],
                    axis=1,
                )
            acc_ref[at] = acc_ref[at] * shrinks[at] + fresh

        share = per * len(tiles)
        expand_keys(0)
        product(0)
        expand_values(0)
        for at in range(len(work) + 1):
            ahead = (at + 3) // share
            if (at + 3) % share == 0 and 0 < ahead < parcels:
                expand_keys(ahead)
            ahead = (at + 1) // share
            if (at + 1) % share == 0 and 0 < ahead < parcels:
                expand_values(ahead)
            if at + 1 < len(work):
                product(at + 1)
            if at < len(work):
                soften(at)
            if at > 0:
                weigh(at - 1)

    if first:
        visit(0, True)

    @pl.loop(1 if first else 0, blocks)
    def each_block(block):
        low = 2 * block - (1 if first else 0)
        high = jnp.minimum(low + 1, slot - 1)

        @pl.when((vis_ref[low] > 0) | (vis_ref[high] > 0))
        def seen():
            visit(block, False)

    if last:
        for pair in range(pairs):
            pieces_of = ([], [])
            for i, (_, parts) in enumerate(tiles):
                done = acc_ref[pair * len(tiles) + i]
                done = done[:VALUE_DIM] / done[VALUE_DIM : VALUE_DIM + 1]
                for side, low, high in parts:
                    pieces_of[side].append(done[:, low:high])
            both = jnp.concatenate([jnp.concatenate(p, axis=1) for p in pieces_of], axis=0)
            out_ref[:, pair * 2 * VALUE_DIM : (pair + 1) * 2 * VALUE_DIM] = both.T.astype(out_ref.dtype)


def attention_stage(visible, queries_t, query_rot_t, key_up, value_up, slots, rows, groups,
                    own=None, state=None, last=False):
    first = own is not None
    heads = key_up.shape[1] // NOPE_DIM
    tok_rows = queries_t.shape[1]
    counts = [[p.shape[0] if p.ndim == 3 else 0 for p in s] for s in slots]
    total_blocks = sum(c[0] or 1 for c in counts) + (1 if first else 0)
    blocks = (total_blocks + 1) // 2
    width, tiles = tiles_of(tok_rows)
    tile_count = heads // 2 * len(tiles)
    extra = own if first else state
    consts = [queries_t, query_rot_t, key_up, value_up]
    flat = [p for s in slots for p in s]
    acc_shape = (tile_count, VALUE_DIM + SUM_ROWS, width)
    max_shape = (tile_count, width)
    parcels = max(1, heads // 4)
    keys = 2 * tok_rows
    scratch = (
        [
            pltpu.VMEM((blocks, keys, key_up.shape[0]), jnp.bfloat16),
            pltpu.VMEM((blocks, keys, 128), jnp.bfloat16),
            pltpu.VMEM((heads // 2, 256, 2 * tok_rows), jnp.bfloat16),
            pltpu.VMEM(value_up.shape[::-1], jnp.bfloat16),
        ]
        + [pltpu.VMEM((keys, width), jnp.float32)] * 2
        + [pltpu.VMEM((keys, width), jnp.bfloat16)] * 2
        + [pltpu.VMEM((keys, heads // parcels * NOPE_DIM), jnp.bfloat16)] * parcels
        + [pltpu.VMEM((heads // parcels * (VALUE_DIM + SUM_ROWS), keys), jnp.bfloat16)] * parcels
    )
    if last:
        out_shape = jax.ShapeDtypeStruct((tok_rows, heads * VALUE_DIM), jnp.bfloat16)
        scratch = [pltpu.VMEM(max_shape, jnp.float32), pltpu.VMEM(acc_shape, jnp.float32)] + scratch
    else:
        out_shape = (
            jax.ShapeDtypeStruct(max_shape, jnp.float32),
            jax.ShapeDtypeStruct(acc_shape, jnp.float32),
        )
    flops = 2 * total_blocks * tok_rows * tok_rows * heads * (256 + VALUE_DIM)
    in_vmem = pl.BlockSpec()
    return pl.pallas_call(
        functools.partial(attention_kernel, first, last, counts, rows, groups, heads),
        in_specs=[pl.BlockSpec(memory_space=pltpu.SMEM)] + [in_vmem] * (len(consts) + len(flat) + len(extra)),
        out_specs=in_vmem if last else (in_vmem, in_vmem),
        scratch_shapes=scratch,
        out_shape=out_shape,
        compiler_params=pltpu.CompilerParams(vmem_limit_bytes=24 * 1024 * 1024),
        cost_estimate=pl.CostEstimate(
            flops=flops, bytes_accessed=4 << 20, transcendentals=total_blocks * tok_rows * tok_rows * heads
        ),
        name="attention_first" if first else "attention_rest",
    )(visible, *consts, *flat, *extra)


def conv_kernel(rim, gated_ref, rim_ref, taps_ref, out_ref, padded_ref):
    rows, chans = gated_ref.shape
    padded_ref[:rim, :] = rim_ref[...].astype(jnp.float32)
    padded_ref[rim : rim + rows, :] = gated_ref[...].astype(jnp.float32)
    offset = rim - (KERNEL - 1)
    step = math.gcd(rows, 64)
    for lane in range(0, chans, 128):
        lanes = slice(lane, lane + 128)
        for row in range(0, rows, step):
            acc = jnp.zeros((step, 128), jnp.float32)
            for phase in range(8):
                taps = range(phase, KERNEL, 8)
                start = row + offset + phase
                part = padded_ref[start : start + step + 8 * (len(taps) - 1), lanes]
                for j, tap in enumerate(taps):
                    acc = acc + taps_ref[tap : tap + 1, lanes] * part[8 * j : 8 * j + step]
            out_ref[row : row + step, lanes] = acc


def convolve(gated, rim, taps):
    rows, chans = gated.shape
    rim_rows = rim.shape[0]
    return pl.pallas_call(
        functools.partial(conv_kernel, rim_rows),
        out_shape=jax.ShapeDtypeStruct((rows, chans), jnp.float32),
        scratch_shapes=[pltpu.VMEM((rim_rows + rows, chans), jnp.float32)],
        compiler_params=pltpu.CompilerParams(vmem_limit_bytes=6 * 1024 * 1024),
        cost_estimate=pl.CostEstimate(
            flops=2 * KERNEL * rows * chans * 50, bytes_accessed=6 * rows * chans, transcendentals=0
        ),
        name="conv",
    )(gated, rim, taps)


def shards(
    tokens,
    input_gain,
    query_weight,
    query_rot_weight,
    kv_down,
    rot_down,
    kv_gain,
    key_up,
    value_up,
    conv_value_weight,
    conv_gate_weight,
    conv_taps,
    conv_ln_gain,
    conv_ln_bias,
    att_out_gain,
    conv_out_gain,
    att_out_weight,
    conv_out_weight,
):
    tok_rows = tokens.shape[0]
    heads_here = key_up.shape[1] // NOPE_DIM
    tp_size, sp_size = lax.axis_size("tp"), lax.axis_size("sp")
    tp_index, sp_index = lax.axis_index("tp"), lax.axis_index("sp")
    f32, bf16 = jnp.float32, jnp.bfloat16

    positions = sp_index * tok_rows + jnp.arange(tok_rows, dtype=jnp.int32)
    cos_table, sine_table = rotary_tables(positions, ROT_DIM // 2)

    rows = tok_rows // tp_size
    rank = kv_down.shape[1]
    groups = max(
        g for g in range(1, rank // ROT_DIM + 1) if rows % g == 0 and (rows // g) % 8 == 0
    )
    scaled, row_scale, latent, own_rot, mine = front(
        jnp.full((1,), tp_index, jnp.int32),
        [tokens] + others(tokens, "tp"),
        input_gain[None, :],
        kv_down,
        rot_down.T,
        kv_gain[None, :],
        jnp.concatenate([cos_table, cos_table], axis=1),
        jnp.concatenate([-sine_table, sine_table], axis=1),
        groups,
    )

    plane = 4 if sp_size % 4 == 0 else 1
    high, low = sp_index // plane, sp_index % plane
    far = range(1, sp_size // plane)
    near, column = [], []
    for b in range(1, plane):
        near.append(swap_bits(mine, "sp", b))
    for s in far:
        column.append(shift_by(mine, "sp", plane * s))
    near_vis = [((low ^ b) < low).astype(jnp.int32) for b in range(1, plane)]
    column_vis = [(high >= s).astype(jnp.int32) for s in far]

    def with_pieces(arrays):
        return [[a] + others(a, "tp") for a in arrays]

    def project(weight):
        return jnp.dot(scaled, weight, preferred_element_type=f32)

    gated = (
        project(conv_value_weight) * row_scale * jax.nn.sigmoid(project(conv_gate_weight) * row_scale)
    ).astype(bf16)
    rim_rows = 32
    rim = shift_by(gated[tok_rows - rim_rows :], "sp", 1)
    scaled, gated = lax.optimization_barrier((scaled, gated))
    query_scale = row_scale * (math.log2(math.e) / math.sqrt(NOPE_DIM + ROT_DIM))
    queries_t = (project(query_weight) * query_scale).astype(bf16).T
    query_rot_t = (
        rotate_half(
            (project(query_rot_weight) * query_scale).reshape(tok_rows, heads_here, ROT_DIM),
            cos_table[:, None, :],
            sine_table[:, None, :],
        )
        .astype(bf16)
        .reshape(tok_rows, heads_here * ROT_DIM)
        .T
    )
    gated, rim, queries_t, query_rot_t = lax.optimization_barrier((gated, rim, queries_t, query_rot_t))
    conv_out = convolve(gated, rim, conv_taps)
    moments = total(jnp.stack([jnp.sum(conv_out, axis=1), jnp.sum(conv_out * conv_out, axis=1)]), "tp")
    mean_val = moments[0] / CONV_CH
    spread = moments[1] / CONV_CH - mean_val * mean_val
    normed = (conv_out - mean_val[:, None]) * lax.rsqrt(spread + norm_eps)[:, None]
    swished = jax.nn.silu(normed * conv_ln_gain[None, :] + conv_ln_bias[None, :])
    conv_sq = total(jnp.sum(swished * swished, axis=1)[None, :], "tp")[0]
    conv_mixed = (
        swished * lax.rsqrt(conv_sq / CONV_CH + norm_eps)[:, None] * conv_out_gain[None, :]
    ).astype(bf16)
    width = D_MODEL // tp_size

    def columns_of(device, weight):
        return lax.dynamic_slice_in_dim(weight, device * width, width, 1)

    def scatter(product):
        parts = []
        for d in range(1, tp_size):
            send = product((tp_index + tp_size - d) % tp_size).astype(bf16)
            parts.append(
                lax.ppermute(send, "tp", [((i + d) % tp_size, i) for i in range(tp_size)])
            )
        own = lax.optimization_barrier(product(tp_index))
        return own, parts

    own = (latent, own_rot)
    stage = functools.partial(
        attention_stage,
        queries_t=queries_t,
        query_rot_t=query_rot_t,
        key_up=key_up,
        value_up=value_up,
        rows=rows,
        groups=groups,
    )
    slots_one, vis_one = with_pieces(near + column), near_vis + column_vis
    slots_two, vis_two = [], []
    if plane == 4:
        if len(slots_one) % 2 == 0:
            slots_two, vis_two = slots_one[-1:], vis_one[-1:]
            slots_one, vis_one = slots_one[:-1], vis_one[:-1]
        column_all = jnp.stack(column)
        arrived = []
        for b in (1, 2):
            arrived.append(swap_bits(column_all, "sp", b))
        for s in far:
            arrived.append(shift_by(near[2], "sp", plane * s))
        state = stage(jnp.stack(vis_one), slots=slots_one, own=own)
        state, arrived, conv_mixed = lax.optimization_barrier((state, arrived, conv_mixed))
        slots_two = slots_two + with_pieces(arrived)
        vis_two = vis_two + column_vis * 3
    conv_own, conv_rest = scatter(
        lambda device: jnp.dot(
            conv_mixed, columns_of(device, conv_out_weight), preferred_element_type=f32
        )
    )
    conv_part = conv_own
    for part in conv_rest:
        conv_part = conv_part + part.astype(f32)
    if slots_two:
        state, conv_part = lax.optimization_barrier((state, conv_part))
        attended = stage(jnp.stack(vis_two), slots=slots_two, state=state, last=True)
    else:
        attended = stage(jnp.stack(vis_one), slots=slots_one, own=own, last=True)

    wide_att = attended.astype(f32)
    att_sq = total(jnp.sum(wide_att * wide_att, axis=1)[None, :], "tp")[0]
    gained = (wide_att * att_out_gain[None, :]).astype(bf16)
    att_part, att_rest = scatter(
        lambda device: jnp.dot(gained, columns_of(device, att_out_weight), preferred_element_type=f32)
    )
    for part in att_rest:
        att_part = att_part + part.astype(f32)
    return (att_part * lax.rsqrt(att_sq / ATT_WIDTH + norm_eps)[:, None] + conv_part).astype(bf16)


def solution(mesh):
    return jax.shard_map(
        shards,
        mesh=mesh,
        in_specs=(
            P("sp", "tp"),
            P(),
            P(None, "tp"),
            P(None, "tp"),
            P(),
            P(),
            P(),
            P(None, "tp"),
            P(None, "tp"),
            P(None, "tp"),
            P(None, "tp"),
            P(None, "tp"),
            P("tp"),
            P("tp"),
            P("tp"),
            P("tp"),
            P("tp", None),
            P("tp", None),
        ),
        out_specs=P("sp", "tp"),
        check_vma=False,
    )
```

profile of v0, /device:TPU:21, one launch (start us, length us, event | category | flops | bytes accessed | tf_op | source)
XLA Modules:
  0.0 100.2 jit_solution(12106408855564514437)
XLA Ops:
  1.2 1.6 %collective-permute-done.refs_1_ = bf16[384,1024]{1,0:T(8,128)(2,1)S(1)} collective-permute-done((bf16[384,1024]{1,0:T(8,128)(2,1)}, bf16[384,1024]{1,0:T(8,128)(2,1)S(1)}, u32[]{:S(2)}, u32[]{:S(2)}) %collective-permute-start) | collective-permute-done | bytes 786464 | tf_op jit(solution)/shard_map/ppermute | solution.py:58
  2.8 1.2 %copy-done.1 = bf16[2048,256]{1,0:T(8,128)(2,1)S(1)} copy-done((bf16[2048,256]{1,0:T(8,128)(2,1)S(1)}, bf16[2048,256]{1,0:T(8,128)(2,1)}, u32[]{:S(2)}) %copy-start.1) | copy-done | bytes 1048600
  7.4 2.0 %front.1 = (bf16[384,2048]{1,0:T(8,128)(2,1)S(1)}, f32[384,1]{1,0:T(8,128)S(1)}, bf16[384,256]{1,0:T(8,128)(2,1)S(1)}, bf16[384,128]{1,0:T(8,128)(2,1)S(1)}, bf16[224,256]{1,0:T(8,128)(2,1)S(1)}) custom-call(s32[1]{0:T(128)} %bitcast.3.index_ref, bf16[384,1024]{1,0:T(8,128)(2,1)S(1)} %copy-done.2, bf16[384,1024]{1,0:T(8,128)(2,1)S(1)} %collective-permute-done.refs_1_, ...), custom_call_target="tpu_custom_call" | custom-call | flops 805306368 | bytes 8388608 | tf_op jit(solution)/shard_map/front/pallas_call | solution.py:127
  14.1 2.0 %fusion.14.refs_0_ = bf16[512,384]{1,0:T(8,128)(2,1)} fusion(f32[384]{0:T(512)S(1)} %get-tuple-element.55, bf16[384,2048]{1,0:T(8,128)(2,1)S(1)} %get-tuple-element.32, bf16[2048,512]{1,0:T(8,128)(2,1)S(1)} %copy-done.33), kind=kOutput, calls=%fused_computation.27 | convolution fusion | flops 805699584 | bytes 4064768 | tf_op jit(solution)/shard_map/dot_general | solution.py:499
  16.1 3.1 %collective-permute-start.1 = (bf16[32,512]{1,0:T(8,128)(2,1)S(1)}, bf16[32,512]{1,0:T(8,128)(2,1)S(1)}, u32[]{:S(2)}, u32[]{:S(2)}) collective-permute-start(bf16[32,512]{1,0:T(8,128)(2,1)S(1)} %slice.20), channel_id=1, source_target_pairs={{0,2},{2,4},{4,6},{6,8},{8,10},{10,12},{12,14},{14,16},{16,18},{18... | collective-permute-start | bytes 98312 | tf_op jit(solution)/shard_map/ppermute | solution.py:48
  19.3 2.4 %collective-permute-done.1.rim_ref = bf16[32,512]{1,0:T(8,128)(2,1)S(1)} collective-permute-done((bf16[32,512]{1,0:T(8,128)(2,1)S(1)}, bf16[32,512]{1,0:T(8,128)(2,1)S(1)}, u32[]{:S(2)}, u32[]{:S(2)}) %collective-permute-start.1) | collective-permute-done | bytes 32800 | tf_op jit(solution)/shard_map/ppermute | solution.py:48
  21.7 3.3 %conv.1 = f32[384,512]{1,0:T(8,128)S(1)} custom-call(bf16[384,512]{1,0:T(8,128)(2,1)S(1)} %fusion.5.gated_ref, bf16[32,512]{1,0:T(8,128)(2,1)S(1)} %collective-permute-done.1.rim_ref, f32[31,512]{1,0:T(8,128)S(1)} %copy-done.19), custom_call_target="tpu_custom_call" | custom-call | flops 609484800 | bytes 1179648 | tf_op jit(solution)/shard_map/conv/pallas_call | solution.py:426
  25.2 1.6 %collective-permute-start.19 = (f32[2,384]{1,0:T(2,128)S(1)}, f32[2,384]{1,0:T(2,128)S(1)}, u32[]{:S(2)}, u32[]{:S(2)}) collective-permute-start(f32[2,384]{1,0:T(2,128)S(1)} %pad_maximum_fusion.4), channel_id=1, source_target_pairs={{1,0},{0,1},{3,2},{2,3},{5,4},{4,5},{7,6},{6,7},{9,8},{8,9},{11,10... | collective-permute-start | bytes 9224 | tf_op jit(solution)/shard_map/ppermute | solution.py:58
  27.7 1.3 %multiply_reduce_fusion = (f32[384]{0:T(512)S(1)}, f32[384,512]{1,0:T(8,128)}) fusion(f32[512]{0:T(512)S(1)} %copy-done.27, f32[512]{0:T(512)S(1)} %copy-done.28, f32[384]{0:T(512)S(1)} %add_rsqrt_fusion, f32[384,512]{1,0:T(8,128)S(1)} %conv.1, f32[384]{0:T(512)S(1)} %get-tuple-element.57), kind=kLoop, calls=%fused_computation.23 | loop fusion | flops 1965696 | bytes 1581568 | tf_op jit(solution)/shard_map/reduce_sum | solution.py:526
  29.4 3.2 %collective-permute-start.10 = (bf16[224,256]{1,0:T(8,128)(2,1)S(1)}, bf16[224,256]{1,0:T(8,128)(2,1)S(1)}, u32[]{:S(2)}, u32[]{:S(2)}) collective-permute-start(bf16[224,256]{1,0:T(8,128)(2,1)S(1)} %get-tuple-element.35), channel_id=1, source_target_pairs={{0,8},{2,10},{4,12},{6,14},{8,16},{10,18},{12,20},{14,22},{16,24},... | collective-permute-start | bytes 344072 | tf_op jit(solution)/shard_map/ppermute | solution.py:48
  32.6 1.3 %collective-permute-start.12 = (bf16[224,256]{1,0:T(8,128)(2,1)S(1)}, bf16[224,256]{1,0:T(8,128)(2,1)S(1)}, u32[]{:S(2)}, u32[]{:S(2)}) collective-permute-start(bf16[224,256]{1,0:T(8,128)(2,1)S(1)} %get-tuple-element.35), channel_id=1, source_target_pairs={{0,16},{2,18},{4,20},{6,22},{8,24},{10,26},{12,28},{14,30},{1,17},... | collective-permute-start | bytes 344072 | tf_op jit(solution)/shard_map/ppermute | solution.py:48
  33.9 1.6 %collective-permute-start.4 = (bf16[224,256]{1,0:T(8,128)(2,1)S(1)}, bf16[224,256]{1,0:T(8,128)(2,1)S(1)}, u32[]{:S(2)}, u32[]{:S(2)}) collective-permute-start(bf16[224,256]{1,0:T(8,128)(2,1)S(1)} %get-tuple-element.35), channel_id=1, source_target_pairs={{0,2},{2,0},{4,6},{6,4},{8,10},{10,8},{12,14},{14,12},{16,18},{18,... | collective-permute-start | bytes 344072 | tf_op jit(solution)/shard_map/ppermute | solution.py:52
  36.5 1.3 %multiply_convert_fusion = bf16[384,512]{1,0:T(8,128)(2,1)S(1)} fusion(f32[384,512]{1,0:T(8,128)} %get-tuple-element.60, f32[512]{0:T(512)S(1)} %copy-done.29, f32[384]{0:T(512)S(1)} %rsqrt_reduce_fusion.1), kind=kLoop, calls=%fused_computation.22 | loop fusion | flops 589824 | bytes 1183232 | tf_op jit(solution)/shard_map/convert_element_type | solution.py:529
  39.7 1.4 %collective-permute-start.11 = (bf16[224,256]{1,0:T(8,128)(2,1)S(1)}, bf16[224,256]{1,0:T(8,128)(2,1)S(1)}, u32[]{:S(2)}, u32[]{:S(2)}) collective-permute-start(bf16[224,256]{1,0:T(8,128)(2,1)S(1)} %collective-permute-done.10.refs_10_), channel_id=1, source_target_pairs={{1,0},{0,1},{3,2},{2,3},{5,4},{4,5},{7,6},{6,7},{9,8},{8,9},{11,10... | collective-permute-start | bytes 344072 | tf_op jit(solution)/shard_map/ppermute | solution.py:58
  41.7 1.6 %collective-permute-start.14 = (bf16[3,224,256]{2,1,0:T(8,128)(2,1)S(1)}, bf16[3,224,256]{2,1,0:T(8,128)(2,1)S(1)}, u32[]{:S(2)}, u32[]{:S(2)}) collective-permute-start(bf16[3,224,256]{2,1,0:T(8,128)(2,1)S(1)} %pad_maximum_fusion), channel_id=1, source_target_pairs={{0,2},{2,0},{4,6},{6,4},{8,10},{10,8},{12,14},{14,12},{16,18},{18,... | collective-permute-start | bytes 1032200 | tf_op jit(solution)/shard_map/ppermute | solution.py:52
  43.6 6.3 %collective-permute-start.16 = (bf16[224,256]{1,0:T(8,128)(2,1)S(1)}, bf16[224,256]{1,0:T(8,128)(2,1)S(1)}, u32[]{:S(2)}, u32[]{:S(2)}) collective-permute-start(bf16[224,256]{1,0:T(8,128)(2,1)S(1)} %collective-permute-done.8.refs_8_), channel_id=1, source_target_pairs={{0,8},{2,10},{4,12},{6,14},{8,16},{10,18},{12,20},{14,22},{16,24},... | collective-permute-start | bytes 344072 | tf_op jit(solution)/shard_map/ppermute | solution.py:48
  49.9 1.3 %collective-permute-start.17 = (bf16[224,256]{1,0:T(8,128)(2,1)S(1)}, bf16[224,256]{1,0:T(8,128)(2,1)S(1)}, u32[]{:S(2)}, u32[]{:S(2)}) collective-permute-start(bf16[224,256]{1,0:T(8,128)(2,1)S(1)} %collective-permute-done.8.refs_8_), channel_id=1, source_target_pairs={{0,16},{2,18},{4,20},{6,22},{8,24},{10,26},{12,28},{14,30},{1,17},... | collective-permute-start | bytes 344072 | tf_op jit(solution)/shard_map/ppermute | solution.py:48
  55.9 11.1 %attention_first.1 = (f32[12,256]{1,0:T(8,128)S(1)}, f32[12,80,256]{2,1,0:T(8,128)S(1)}) custom-call(s32[5]{0:T(128)S(1)} %stack.85.vis_ref, bf16[512,384]{1,0:T(8,128)(2,1)S(1)} %copy-done.20, bf16[256,384]{1,0:T(8,128)(2,1)S(1)} %bitcast.29, bf16[256,512]{1,0:T(8,128)(2,1)S(1)} %copy-done.6, bf16[256,512]{1,0:T(8,128)(2,1)S(1)} %copy-done.7, ...), custom_call_target="tpu_custom_call" | custom-call | flops 4529848320 | bytes 4194304 | tf_op jit(solution)/shard_map/attention_first/pallas_call | solution.py:390
  68.7 1.5 %convolution_convert_fusion.1 = bf16[384,1024]{1,0:T(8,128)(2,1)} fusion(bf16[384,512]{1,0:T(8,128)(2,1)S(1)} %multiply_convert_fusion, bf16[512,2048]{1,0:T(8,128)(2,1)S(1)} %copy-done, s32[]{:T(128)S(6)} %select_n.29), kind=kOutput, calls=%fused_computation.3 | convolution fusion | flops 403046400 | bytes 2228228 | tf_op jit(solution)/shard_map/dot_general | solution.py:572
  70.2 1.3 %collective-permute-start.26 = (bf16[384,1024]{1,0:T(8,128)(2,1)}, bf16[384,1024]{1,0:T(8,128)(2,1)}, u32[]{:S(2)}, u32[]{:S(2)}) collective-permute-start(bf16[384,1024]{1,0:T(8,128)(2,1)} %convolution_convert_fusion.1), channel_id=1, source_target_pairs={{1,0},{0,1},{3,2},{2,3},{5,4},{4,5},{7,6},{6,7},{9,8},{8,9},{11,10... | collective-permute-start | bytes 2359304 | tf_op jit(solution)/shard_map/ppermute | solution.py:540
  72.2 1.6 %fusion.10 = f32[384,1024]{1,0:T(8,128)S(1)} fusion(bf16[384,512]{1,0:T(8,128)(2,1)} %copy-done.24, bf16[512,2048]{1,0:T(8,128)(2,1)S(1)} %copy-done, s32[]{:T(128)S(6)} %select_n.27), kind=kOutput, calls=%fused_computation.16 | convolution fusion | flops 402653184 | bytes 3014660 | tf_op jit(solution)/shard_map/dot_general | solution.py:572
  74.8 1.4 %convert_add_fusion = f32[384,1024]{1,0:T(8,128)S(1)} fusion(f32[384,1024]{1,0:T(8,128)S(1)} %fusion.10, bf16[384,1024]{1,0:T(8,128)(2,1)} %collective-permute-done.26), kind=kLoop, calls=%fused_computation.1 | loop fusion | flops 786432 | bytes 3932160 | tf_op jit(solution)/shard_map/add | solution.py:578
  76.3 19.7 %attention_rest.1 = bf16[384,512]{1,0:T(8,128)(2,1)S(1)} custom-call(s32[10]{0:T(128)S(1)} %stack.78.vis_ref, bf16[512,384]{1,0:T(8,128)(2,1)S(1)} %copy-done.21, bf16[256,384]{1,0:T(8,128)(2,1)S(1)} %bitcast.30, bf16[256,512]{1,0:T(8,128)(2,1)S(1)} %copy-done.6, bf16[256,512]{1,0:T(8,128)(2,1)S(1)} %copy-done.8, ...), custom_call_target="tpu_custom_call" | custom-call | flops 7549747200 | bytes 4194304 | tf_op jit(solution)/shard_map/attention_rest/pallas_call | solution.py:390
  99.0 1.2 %add_convert_fusion = bf16[384,1024]{1,0:T(8,128)(2,1)} fusion(f32[384,1024]{1,0:T(8,128)S(1)} %convert_add_fusion, f32[384,1024]{1,0:T(8,128)S(1)} %fusion.7, bf16[384,1024]{1,0:T(8,128)(2,1)S(1)} %collective-permute-done.27, f32[384]{0:T(512)S(1)} %rsqrt_reduce_fusion), kind=kLoop, calls=%fused_computation | loop fusion | flops 1966080 | bytes 4720128 | tf_op jit(solution)/shard_map/convert_element_type | solution.py:593
  (143 shorter events, 25.4 us)
Async XLA Ops:
  0.0 2.8 %collective-permute-start = (bf16[384,1024]{1,0:T(8,128)(2,1)}, bf16[384,1024]{1,0:T(8,128)(2,1)S(1)}, u32[]{:S(2)}, u32[]{:S(2)}) collective-permute-start(bf16[384,1024]{1,0:T(8,128)(2,1)} %refs_0_.1), channel_id=1, source_target_pairs={{1,0},{0,1},{3,2},{2,3},{5,4},{4,5},{7,6},{6,7},{9,8},{8,9},{11,10... | collective-permute-start | bytes 2359304 | tf_op jit(solution)/shard_map/ppermute | solution.py:58
  16.1 5.5 %collective-permute-start.1 = (bf16[32,512]{1,0:T(8,128)(2,1)S(1)}, bf16[32,512]{1,0:T(8,128)(2,1)S(1)}, u32[]{:S(2)}, u32[]{:S(2)}) collective-permute-start(bf16[32,512]{1,0:T(8,128)(2,1)S(1)} %slice.20), channel_id=1, source_target_pairs={{0,2},{2,4},{4,6},{6,8},{8,10},{10,12},{12,14},{14,16},{16,18},{18... | collective-permute-start | bytes 98312 | tf_op jit(solution)/shard_map/ppermute | solution.py:48
  26.8 9.1 %collective-permute-start.8 = (bf16[224,256]{1,0:T(8,128)(2,1)S(1)}, bf16[224,256]{1,0:T(8,128)(2,1)S(1)}, u32[]{:S(2)}, u32[]{:S(2)}) collective-permute-start(bf16[224,256]{1,0:T(8,128)(2,1)S(1)} %get-tuple-element.35), channel_id=1, source_target_pairs={{0,6},{2,4},{4,2},{6,0},{8,14},{10,12},{12,10},{14,8},{16,22},{18,... | collective-permute-start | bytes 344072 | tf_op jit(solution)/shard_map/ppermute | solution.py:52
  28.9 6.5 %collective-permute-start.20 = (f32[1,384]{1,0:T(1,128)S(1)}, f32[1,384]{1,0:T(1,128)S(1)}, u32[]{:S(2)}, u32[]{:S(2)}) collective-permute-start(f32[1,384]{1,0:T(1,128)S(1)} %broadcast_in_dim.13), channel_id=1, source_target_pairs={{1,0},{0,1},{3,2},{2,3},{5,4},{4,5},{7,6},{6,7},{9,8},{8,9},{11,10... | collective-permute-start | bytes 4616 | tf_op jit(solution)/shard_map/ppermute | solution.py:58
  29.4 8.5 %collective-permute-start.10 = (bf16[224,256]{1,0:T(8,128)(2,1)S(1)}, bf16[224,256]{1,0:T(8,128)(2,1)S(1)}, u32[]{:S(2)}, u32[]{:S(2)}) collective-permute-start(bf16[224,256]{1,0:T(8,128)(2,1)S(1)} %get-tuple-element.35), channel_id=1, source_target_pairs={{0,8},{2,10},{4,12},{6,14},{8,16},{10,18},{12,20},{14,22},{16,24},... | collective-permute-start | bytes 344072 | tf_op jit(solution)/shard_map/ppermute | solution.py:48
  32.6 7.1 %collective-permute-start.12 = (bf16[224,256]{1,0:T(8,128)(2,1)S(1)}, bf16[224,256]{1,0:T(8,128)(2,1)S(1)}, u32[]{:S(2)}, u32[]{:S(2)}) collective-permute-start(bf16[224,256]{1,0:T(8,128)(2,1)S(1)} %get-tuple-element.35), channel_id=1, source_target_pairs={{0,16},{2,18},{4,20},{6,22},{8,24},{10,26},{12,28},{14,30},{1,17},... | collective-permute-start | bytes 344072 | tf_op jit(solution)/shard_map/ppermute | solution.py:48
  33.9 7.2 %collective-permute-start.4 = (bf16[224,256]{1,0:T(8,128)(2,1)S(1)}, bf16[224,256]{1,0:T(8,128)(2,1)S(1)}, u32[]{:S(2)}, u32[]{:S(2)}) collective-permute-start(bf16[224,256]{1,0:T(8,128)(2,1)S(1)} %get-tuple-element.35), channel_id=1, source_target_pairs={{0,2},{2,0},{4,6},{6,4},{8,10},{10,8},{12,14},{14,12},{16,18},{18,... | collective-permute-start | bytes 344072 | tf_op jit(solution)/shard_map/ppermute | solution.py:52
  35.5 5.6 %collective-permute-start.6 = (bf16[224,256]{1,0:T(8,128)(2,1)S(1)}, bf16[224,256]{1,0:T(8,128)(2,1)S(1)}, u32[]{:S(2)}, u32[]{:S(2)}) collective-permute-start(bf16[224,256]{1,0:T(8,128)(2,1)S(1)} %get-tuple-element.35), channel_id=1, source_target_pairs={{0,4},{2,6},{4,0},{6,2},{8,12},{10,14},{12,8},{14,10},{16,20},{18,... | collective-permute-start | bytes 344072 | tf_op jit(solution)/shard_map/ppermute | solution.py:52
  35.9 5.7 %collective-permute-start.2 = (bf16[224,256]{1,0:T(8,128)(2,1)S(1)}, bf16[224,256]{1,0:T(8,128)(2,1)S(1)}, u32[]{:S(2)}, u32[]{:S(2)}) collective-permute-start(bf16[224,256]{1,0:T(8,128)(2,1)S(1)} %get-tuple-element.35), channel_id=1, source_target_pairs={{0,24},{2,26},{4,28},{6,30},{1,25},{3,27},{5,29},{7,31}} | collective-permute-start | bytes 344072 | tf_op jit(solution)/shard_map/ppermute | solution.py:48
  37.8 3.8 %collective-permute-start.9 = (bf16[224,256]{1,0:T(8,128)(2,1)S(1)}, bf16[224,256]{1,0:T(8,128)(2,1)S(1)}, u32[]{:S(2)}, u32[]{:S(2)}) collective-permute-start(bf16[224,256]{1,0:T(8,128)(2,1)S(1)} %collective-permute-done.8.refs_8_), channel_id=1, source_target_pairs={{1,0},{0,1},{3,2},{2,3},{5,4},{4,5},{7,6},{6,7},{9,8},{8,9},{11,10... | collective-permute-start | bytes 344072 | tf_op jit(solution)/shard_map/ppermute | solution.py:58
  39.7 3.6 %collective-permute-start.11 = (bf16[224,256]{1,0:T(8,128)(2,1)S(1)}, bf16[224,256]{1,0:T(8,128)(2,1)S(1)}, u32[]{:S(2)}, u32[]{:S(2)}) collective-permute-start(bf16[224,256]{1,0:T(8,128)(2,1)S(1)} %collective-permute-done.10.refs_10_), channel_id=1, source_target_pairs={{1,0},{0,1},{3,2},{2,3},{5,4},{4,5},{7,6},{6,7},{9,8},{8,9},{11,10... | collective-permute-start | bytes 344072 | tf_op jit(solution)/shard_map/ppermute | solution.py:58
  41.0 2.6 %collective-permute-start.13 = (bf16[224,256]{1,0:T(8,128)(2,1)S(1)}, bf16[224,256]{1,0:T(8,128)(2,1)S(1)}, u32[]{:S(2)}, u32[]{:S(2)}) collective-permute-start(bf16[224,256]{1,0:T(8,128)(2,1)S(1)} %collective-permute-done.12.refs_12_), channel_id=1, source_target_pairs={{1,0},{0,1},{3,2},{2,3},{5,4},{4,5},{7,6},{6,7},{9,8},{8,9},{11,10... | collective-permute-start | bytes 344072 | tf_op jit(solution)/shard_map/ppermute | solution.py:58
  41.0 8.9 %collective-permute-start.5 = (bf16[224,256]{1,0:T(8,128)(2,1)S(1)}, bf16[224,256]{1,0:T(8,128)(2,1)S(1)}, u32[]{:S(2)}, u32[]{:S(2)}) collective-permute-start(bf16[224,256]{1,0:T(8,128)(2,1)S(1)} %collective-permute-done.4.refs_4_), channel_id=1, source_target_pairs={{1,0},{0,1},{3,2},{2,3},{5,4},{4,5},{7,6},{6,7},{9,8},{8,9},{11,10... | collective-permute-start | bytes 344072 | tf_op jit(solution)/shard_map/ppermute | solution.py:58
  41.6 9.7 %collective-permute-start.7 = (bf16[224,256]{1,0:T(8,128)(2,1)S(1)}, bf16[224,256]{1,0:T(8,128)(2,1)S(1)}, u32[]{:S(2)}, u32[]{:S(2)}) collective-permute-start(bf16[224,256]{1,0:T(8,128)(2,1)S(1)} %collective-permute-done.6.refs_6_), channel_id=1, source_target_pairs={{1,0},{0,1},{3,2},{2,3},{5,4},{4,5},{7,6},{6,7},{9,8},{8,9},{11,10... | collective-permute-start | bytes 344072 | tf_op jit(solution)/shard_map/ppermute | solution.py:58
  41.7 26.3 %collective-permute-start.14 = (bf16[3,224,256]{2,1,0:T(8,128)(2,1)S(1)}, bf16[3,224,256]{2,1,0:T(8,128)(2,1)S(1)}, u32[]{:S(2)}, u32[]{:S(2)}) collective-permute-start(bf16[3,224,256]{2,1,0:T(8,128)(2,1)S(1)} %pad_maximum_fusion), channel_id=1, source_target_pairs={{0,2},{2,0},{4,6},{6,4},{8,10},{10,8},{12,14},{14,12},{16,18},{18,... | collective-permute-start | bytes 1032200 | tf_op jit(solution)/shard_map/ppermute | solution.py:52
  43.3 24.7 %collective-permute-start.15 = (bf16[3,224,256]{2,1,0:T(8,128)(2,1)S(1)}, bf16[3,224,256]{2,1,0:T(8,128)(2,1)S(1)}, u32[]{:S(2)}, u32[]{:S(2)}) collective-permute-start(bf16[3,224,256]{2,1,0:T(8,128)(2,1)S(1)} %pad_maximum_fusion), channel_id=1, source_target_pairs={{0,4},{2,6},{4,0},{6,2},{8,12},{10,14},{12,8},{14,10},{16,20},{18,... | collective-permute-start | bytes 1032200 | tf_op jit(solution)/shard_map/ppermute | solution.py:52
  43.6 24.4 %collective-permute-start.16 = (bf16[224,256]{1,0:T(8,128)(2,1)S(1)}, bf16[224,256]{1,0:T(8,128)(2,1)S(1)}, u32[]{:S(2)}, u32[]{:S(2)}) collective-permute-start(bf16[224,256]{1,0:T(8,128)(2,1)S(1)} %collective-permute-done.8.refs_8_), channel_id=1, source_target_pairs={{0,8},{2,10},{4,12},{6,14},{8,16},{10,18},{12,20},{14,22},{16,24},... | collective-permute-start | bytes 344072 | tf_op jit(solution)/shard_map/ppermute | solution.py:48
  49.9 18.1 %collective-permute-start.17 = (bf16[224,256]{1,0:T(8,128)(2,1)S(1)}, bf16[224,256]{1,0:T(8,128)(2,1)S(1)}, u32[]{:S(2)}, u32[]{:S(2)}) collective-permute-start(bf16[224,256]{1,0:T(8,128)(2,1)S(1)} %collective-permute-done.8.refs_8_), channel_id=1, source_target_pairs={{0,16},{2,18},{4,20},{6,22},{8,24},{10,26},{12,28},{14,30},{1,17},... | collective-permute-start | bytes 344072 | tf_op jit(solution)/shard_map/ppermute | solution.py:48
  51.2 16.8 %collective-permute-start.18 = (bf16[224,256]{1,0:T(8,128)(2,1)S(1)}, bf16[224,256]{1,0:T(8,128)(2,1)S(1)}, u32[]{:S(2)}, u32[]{:S(2)}) collective-permute-start(bf16[224,256]{1,0:T(8,128)(2,1)S(1)} %collective-permute-done.8.refs_8_), channel_id=1, source_target_pairs={{0,24},{2,26},{4,28},{6,30},{1,25},{3,27},{5,29},{7,31}} | collective-permute-start | bytes 344072 | tf_op jit(solution)/shard_map/ppermute | solution.py:48
  70.2 4.2 %collective-permute-start.26 = (bf16[384,1024]{1,0:T(8,128)(2,1)}, bf16[384,1024]{1,0:T(8,128)(2,1)}, u32[]{:S(2)}, u32[]{:S(2)}) collective-permute-start(bf16[384,1024]{1,0:T(8,128)(2,1)} %convolution_convert_fusion.1), channel_id=1, source_target_pairs={{1,0},{0,1},{3,2},{2,3},{5,4},{4,5},{7,6},{6,7},{9,8},{8,9},{11,10... | collective-permute-start | bytes 2359304 | tf_op jit(solution)/shard_map/ppermute | solution.py:540
  71.5 2.8 %collective-permute-start.3 = (bf16[224,256]{1,0:T(8,128)(2,1)S(1)}, bf16[224,256]{1,0:T(8,128)(2,1)S(1)}, u32[]{:S(2)}, u32[]{:S(2)}) collective-permute-start(bf16[224,256]{1,0:T(8,128)(2,1)S(1)} %collective-permute-done.2.refs_4_), channel_id=1, source_target_pairs={{1,0},{0,1},{3,2},{2,3},{5,4},{4,5},{7,6},{6,7},{9,8},{8,9},{11,10... | collective-permute-start | bytes 344072 | tf_op jit(solution)/shard_map/ppermute | solution.py:58
  71.6 4.6 %collective-permute-start.21 = (bf16[3,224,256]{2,1,0:T(8,128)(2,1)S(1)}, bf16[3,224,256]{2,1,0:T(8,128)(2,1)S(1)}, u32[]{:S(2)}, u32[]{:S(2)}) collective-permute-start(bf16[3,224,256]{2,1,0:T(8,128)(2,1)S(1)} %collective-permute-done.14.refs_6_), channel_id=1, source_target_pairs={{1,0},{0,1},{3,2},{2,3},{5,4},{4,5},{7,6},{6,7},{9,8},{8,9},{11,10... | collective-permute-start | bytes 1032200 | tf_op jit(solution)/shard_map/ppermute | solution.py:58
  72.1 4.2 %collective-permute-start.22 = (bf16[3,224,256]{2,1,0:T(8,128)(2,1)S(1)}, bf16[3,224,256]{2,1,0:T(8,128)(2,1)S(1)}, u32[]{:S(2)}, u32[]{:S(2)}) collective-permute-start(bf16[3,224,256]{2,1,0:T(8,128)(2,1)S(1)} %collective-permute-done.15.refs_8_), channel_id=1, source_target_pairs={{1,0},{0,1},{3,2},{2,3},{5,4},{4,5},{7,6},{6,7},{9,8},{8,9},{11,10... | collective-permute-start | bytes 1032200 | tf_op jit(solution)/shard_map/ppermute | solution.py:58
  73.8 2.4 %collective-permute-start.23 = (bf16[224,256]{1,0:T(8,128)(2,1)S(1)}, bf16[224,256]{1,0:T(8,128)(2,1)S(1)}, u32[]{:S(2)}, u32[]{:S(2)}) collective-permute-start(bf16[224,256]{1,0:T(8,128)(2,1)S(1)} %copy-done.12), channel_id=1, source_target_pairs={{1,0},{0,1},{3,2},{2,3},{5,4},{4,5},{7,6},{6,7},{9,8},{8,9},{11,10... | collective-permute-start | bytes 344072 | tf_op jit(solution)/shard_map/ppermute | solution.py:58
  (39 other events, 242.9 us)
where the time goes:
time: 101 us; the launch traced here: 100 us
  Pallas kernels  36.1 us (36%)
  starting transfers between devices  30 us (30%)
  local copies, waits for them, and re-layouts  11.9 us (12%)
  matrix products  9.09 us (9%)
  waiting for transfers between devices  6.46 us (6%)
  other arithmetic  6 us (6%)
    pallas_call x2, Pallas kernels, attention_stage(): pl.pallas_call(functools.partial(attention_kernel, first, last, counts, r...  30.8 us
    ppermute x7, starting transfers between devices, shift_by(): lax.ppermute(block, axis, [(i, i + distance) for i in devices if i + dist...  16.7 us
    unnamed x68, local copies, waits for them, and re-layouts  11.5 us
    ppermute x15, starting transfers between devices, others(): lax.ppermute(block, axis, [((i + d) % size, i) for i in range(size)])  7.71 us
    dot_general x4, matrix products, project(): return jnp.dot(scaled, weight, preferred_element_type=f32)  4.89 us
    ppermute x5, starting transfers between devices, swap_bits(): lax.ppermute(block, axis, [(i, i ^ bits) for i in range(lax.axis_size(axi...  4.13 us
    pallas_call x1, Pallas kernels, convolve(): pl.pallas_call(functools.partial(conv_kernel, rim_rows), out_shape=jax.Sh...  3.27 us
    ppermute x7, waiting for transfers between devices, shift_by(): lax.ppermute(block, axis, [(i, i + distance) for i in devices if i + dist...  3.22 us
  transfers between devices with their start and end apart: 29, of which 5 were waited for; matrix products, arithmetic and copies ran while one was open for 7% of the time, Pallas kernels for 11%

commit v1 on v0

--- a/solution.py
+++ b/solution.py
@@ -175,8 +175,8 @@
         (out_ref, max_ref, acc_ref), refs = refs[:3], refs[3:]
     else:
         (max_ref, acc_ref), refs = refs[:2], refs[2:]
-    lat_ref, rot_ref, qbd_ref, turned_ref, score_refs, weight_refs, refs = (
-        refs[0], refs[1], refs[2], refs[3], refs[4:6], refs[6:8], refs[8:]
+    lat_ref, rot_ref, qbd_ref, score_refs, weight_refs, refs = (
+        refs[0], refs[1], refs[2], refs[3:5], refs[5:7], refs[7:]
     )
     pairs = heads // 2
     parcels = max(1, pairs // 2)
@@ -188,7 +188,6 @@
     blocks = lat_ref.shape[0]
     bias_row = 2 * NOPE_DIM + ROT_DIM
 
-    turned_ref[...] = value_up_ref[...].T
     qbd_ref[...] = jnp.zeros_like(qbd_ref)
     for pair in range(pairs):
         qbd_ref[pair, bias_row : bias_row + 16, :] = (
@@ -250,7 +249,7 @@
 
         def expand_values(n):
             values = lax.dot_general(
-                turned_ref[n * span : (n + 1) * span, :],
+                value_up_ref[n * span : (n + 1) * span, :],
                 lat_ref[block],
                 (((1,), (1,)), ((), ())),
                 preferred_element_type=jnp.float32,
@@ -370,7 +369,6 @@
             pltpu.VMEM((blocks, keys, key_up.shape[0]), jnp.bfloat16),
             pltpu.VMEM((blocks, keys, 128), jnp.bfloat16),
             pltpu.VMEM((heads // 2, 256, 2 * tok_rows), jnp.bfloat16),
-            pltpu.VMEM(value_up.shape[::-1], jnp.bfloat16),
         ]
         + [pltpu.VMEM((keys, width), jnp.float32)] * 2
         + [pltpu.VMEM((keys, width), jnp.bfloat16)] * 2
@@ -469,13 +467,20 @@
     groups = max(
         g for g in range(1, rank // ROT_DIM + 1) if rows % g == 0 and (rows // g) % 8 == 0
     )
+
+    def near_by(array):
+        return jnp.maximum(array, jnp.finfo(array.dtype).min)
+
+    token_pieces = others(tokens, "tp")
+    key_up = near_by(key_up)
+    value_up = value_up.T
     scaled, row_scale, latent, own_rot, mine = front(
         jnp.full((1,), tp_index, jnp.int32),
-        [tokens] + others(tokens, "tp"),
-        input_gain[None, :],
-        kv_down,
-        rot_down.T,
-        kv_gain[None, :],
+        [near_by(tokens)] + token_pieces,
+        near_by(input_gain)[None, :],
+        near_by(kv_down),
+        near_by(rot_down.T),
+        near_by(kv_gain)[None, :],
         jnp.concatenate([cos_table, cos_table], axis=1),
         jnp.concatenate([-sine_table, sine_table], axis=1),
         groups,

time: 101 us -> 98.7 us (0.977)
  local copies, waits for them, and re-layouts: 11.9 us -> 6.57 us
  other arithmetic: 6 us -> 9.71 us
  waiting for transfers between devices: 6.46 us -> 4.54 us
    unnamed x68 -> x53, local copies, waits for them, and re-layouts: 11.5 us -> 6.13 us
    max x0 -> x6, other arithmetic: none -> 3.71 us  [near_by(): return jnp.maximum(array, jnp.finfo(array.dtype).min)]
    ppermute x15, waiting for transfers between devices: 3.22 us -> 1.44 us  [others(): lax.ppermute(block, axis, [((i + d) % size, i) for i in range(size)])]
  transfers between devices with their start and end apart: 29 -> 29, of which waited for: 5 -> 4; matrix products, arithmetic and copies ran while one was open for 7% -> 12% of each run, Pallas kernels for 11% -> 12%
where the time goes in v1:
time: 98.7 us; the launch traced here: 98 us
  Pallas kernels  37 us (37%)
  starting transfers between devices  30.4 us (31%)
  other arithmetic  9.71 us (10%)
  matrix products  9.1 us (9%)
  local copies, waits for them, and re-layouts  6.57 us (7%)
  waiting for transfers between devices  4.54 us (5%)
    pallas_call x2, Pallas kernels, attention_stage(): pl.pallas_call(functools.partial(attention_kernel, first, last, counts, r...  31.7 us
    ppermute x7, starting transfers between devices, shift_by(): lax.ppermute(block, axis, [(i, i + distance) for i in devices if i + dist...  17.1 us
    ppermute x15, starting transfers between devices, others(): lax.ppermute(block, axis, [((i + d) % size, i) for i in range(size)])  7.54 us
    unnamed x53, local copies, waits for them, and re-layouts  6.13 us
    dot_general x4, matrix products, project(): return jnp.dot(scaled, weight, preferred_element_type=f32)  4.9 us
    ppermute x5, starting transfers between devices, swap_bits(): lax.ppermute(block, axis, [(i, i ^ bits) for i in range(lax.axis_size(axi...  4.29 us
    max x6, other arithmetic, near_by(): return jnp.maximum(array, jnp.finfo(array.dtype).min)  3.71 us
    pallas_call x1, Pallas kernels, convolve(): pl.pallas_call(functools.partial(conv_kernel, rim_rows), out_shape=jax.Sh...  3.27 us
  transfers between devices with their start and end apart: 29, of which 4 were waited for; matrix products, arithmetic and copies ran while one was open for 12% of the time, Pallas kernels for 12%

profile of v1, /device:TPU:21, one launch (start us, length us, event | category | flops | bytes accessed | tf_op | source)
XLA Modules:
  0.0 98.0 jit_solution(15472560763530724939)
XLA Ops:
  4.1 1.3 %broadcast_maximum_fusion.1.refs_0_ = bf16[384,1024]{1,0:T(8,128)(2,1)S(1)} fusion(bf16[384,1024]{1,0:T(8,128)(2,1)} %param.18), kind=kLoop, calls=%fused_computation.29 | loop fusion | flops 393216 | bytes 1572864 | tf_op jit(solution)/shard_map/max | solution.py:472
  5.6 2.0 %front.1 = (bf16[384,2048]{1,0:T(8,128)(2,1)S(1)}, f32[384,1]{1,0:T(8,128)S(1)}, bf16[384,256]{1,0:T(8,128)(2,1)S(1)}, bf16[384,128]{1,0:T(8,128)(2,1)S(1)}, bf16[224,256]{1,0:T(8,128)(2,1)S(1)}) custom-call(s32[1]{0:T(128)} %bitcast.3.index_ref, bf16[384,1024]{1,0:T(8,128)(2,1)S(1)} %broadcast_maximum_fusion.1.refs_0_, ...), custom_call_target="tpu_custom_call" | custom-call | flops 805306368 | bytes 8388608 | tf_op jit(solution)/shard_map/front/pallas_call | solution.py:127
  12.3 2.0 %fusion.14.refs_0_ = bf16[512,384]{1,0:T(8,128)(2,1)} fusion(f32[384]{0:T(512)S(1)} %get-tuple-element.55, bf16[384,2048]{1,0:T(8,128)(2,1)S(1)} %get-tuple-element.32, bf16[2048,512]{1,0:T(8,128)(2,1)S(1)} %copy-done.25), kind=kOutput, calls=%fused_computation.28 | convolution fusion | flops 805699584 | bytes 4064768 | tf_op jit(solution)/shard_map/dot_general | solution.py:504
  14.3 3.1 %collective-permute-start.1 = (bf16[32,512]{1,0:T(8,128)(2,1)S(1)}, bf16[32,512]{1,0:T(8,128)(2,1)S(1)}, u32[]{:S(2)}, u32[]{:S(2)}) collective-permute-start(bf16[32,512]{1,0:T(8,128)(2,1)S(1)} %slice.20), channel_id=1, source_target_pairs={{0,2},{2,4},{4,6},{6,8},{8,10},{10,12},{12,14},{14,16},{16,18},{18... | collective-permute-start | bytes 98312 | tf_op jit(solution)/shard_map/ppermute | solution.py:48
  17.5 2.4 %collective-permute-done.1.rim_ref = bf16[32,512]{1,0:T(8,128)(2,1)S(1)} collective-permute-done((bf16[32,512]{1,0:T(8,128)(2,1)S(1)}, bf16[32,512]{1,0:T(8,128)(2,1)S(1)}, u32[]{:S(2)}, u32[]{:S(2)}) %collective-permute-start.1) | collective-permute-done | bytes 32800 | tf_op jit(solution)/shard_map/ppermute | solution.py:48
  19.9 3.3 %conv.1 = f32[384,512]{1,0:T(8,128)S(1)} custom-call(bf16[384,512]{1,0:T(8,128)(2,1)S(1)} %fusion.5.gated_ref, bf16[32,512]{1,0:T(8,128)(2,1)S(1)} %collective-permute-done.1.rim_ref, f32[31,512]{1,0:T(8,128)S(1)} %copy-done.5), custom_call_target="tpu_custom_call" | custom-call | flops 609484800 | bytes 1179648 | tf_op jit(solution)/shard_map/conv/pallas_call | solution.py:424
  23.4 1.4 %collective-permute-start.19 = (f32[2,384]{1,0:T(2,128)S(1)}, f32[2,384]{1,0:T(2,128)S(1)}, u32[]{:S(2)}, u32[]{:S(2)}) collective-permute-start(f32[2,384]{1,0:T(2,128)S(1)} %pad_maximum_fusion.4), channel_id=1, source_target_pairs={{1,0},{0,1},{3,2},{2,3},{5,4},{4,5},{7,6},{6,7},{9,8},{8,9},{11,10... | collective-permute-start | bytes 9224 | tf_op jit(solution)/shard_map/ppermute | solution.py:58
  25.7 1.3 %multiply_reduce_fusion = (f32[384]{0:T(512)S(1)}, f32[384,512]{1,0:T(8,128)}) fusion(f32[512]{0:T(512)S(1)} %copy-done.19, f32[512]{0:T(512)S(1)} %copy-done.20, f32[384]{0:T(512)S(1)} %add_rsqrt_fusion, f32[384,512]{1,0:T(8,128)S(1)} %conv.1, f32[384]{0:T(512)S(1)} %get-tuple-element.57), kind=kLoop, calls=%fused_computation.23 | loop fusion | flops 1965696 | bytes 1581568 | tf_op jit(solution)/shard_map/reduce_sum | solution.py:531
  28.5 3.2 %collective-permute-start.10 = (bf16[224,256]{1,0:T(8,128)(2,1)S(1)}, bf16[224,256]{1,0:T(8,128)(2,1)S(1)}, u32[]{:S(2)}, u32[]{:S(2)}) collective-permute-start(bf16[224,256]{1,0:T(8,128)(2,1)S(1)} %get-tuple-element.35), channel_id=1, source_target_pairs={{0,8},{2,10},{4,12},{6,14},{8,16},{10,18},{12,20},{14,22},{16,24},... | collective-permute-start | bytes 344072 | tf_op jit(solution)/shard_map/ppermute | solution.py:48
  31.7 1.3 %collective-permute-start.12 = (bf16[224,256]{1,0:T(8,128)(2,1)S(1)}, bf16[224,256]{1,0:T(8,128)(2,1)S(1)}, u32[]{:S(2)}, u32[]{:S(2)}) collective-permute-start(bf16[224,256]{1,0:T(8,128)(2,1)S(1)} %get-tuple-element.35), channel_id=1, source_target_pairs={{0,16},{2,18},{4,20},{6,22},{8,24},{10,26},{12,28},{14,30},{1,17},... | collective-permute-start | bytes 344072 | tf_op jit(solution)/shard_map/ppermute | solution.py:48
  33.0 1.6 %collective-permute-start.4 = (bf16[224,256]{1,0:T(8,128)(2,1)S(1)}, bf16[224,256]{1,0:T(8,128)(2,1)S(1)}, u32[]{:S(2)}, u32[]{:S(2)}) collective-permute-start(bf16[224,256]{1,0:T(8,128)(2,1)S(1)} %get-tuple-element.35), channel_id=1, source_target_pairs={{0,2},{2,0},{4,6},{6,4},{8,10},{10,8},{12,14},{14,12},{16,18},{18,... | collective-permute-start | bytes 344072 | tf_op jit(solution)/shard_map/ppermute | solution.py:52
  35.7 1.3 %multiply_convert_fusion = bf16[384,512]{1,0:T(8,128)(2,1)S(1)} fusion(f32[384,512]{1,0:T(8,128)} %get-tuple-element.60, f32[512]{0:T(512)S(1)} %copy-done.21, f32[384]{0:T(512)S(1)} %rsqrt_reduce_fusion.1), kind=kLoop, calls=%fused_computation.22 | loop fusion | flops 589824 | bytes 1183232 | tf_op jit(solution)/shard_map/convert_element_type | solution.py:534
  38.8 1.4 %collective-permute-start.11 = (bf16[224,256]{1,0:T(8,128)(2,1)S(1)}, bf16[224,256]{1,0:T(8,128)(2,1)S(1)}, u32[]{:S(2)}, u32[]{:S(2)}) collective-permute-start(bf16[224,256]{1,0:T(8,128)(2,1)S(1)} %collective-permute-done.10.refs_10_), channel_id=1, source_target_pairs={{1,0},{0,1},{3,2},{2,3},{5,4},{4,5},{7,6},{6,7},{9,8},{8,9},{11,10... | collective-permute-start | bytes 344072 | tf_op jit(solution)/shard_map/ppermute | solution.py:58
  40.8 1.7 %collective-permute-start.14 = (bf16[3,224,256]{2,1,0:T(8,128)(2,1)S(1)}, bf16[3,224,256]{2,1,0:T(8,128)(2,1)}, u32[]{:S(2)}, u32[]{:S(2)}) collective-permute-start(bf16[3,224,256]{2,1,0:T(8,128)(2,1)S(1)} %pad_maximum_fusion), channel_id=1, source_target_pairs={{0,2},{2,0},{4,6},{6,4},{8,10},{10,8},{12,14},{14,12},{16,18},{18,... | collective-permute-start | bytes 1032200 | tf_op jit(solution)/shard_map/ppermute | solution.py:52
  42.8 6.3 %collective-permute-start.16 = (bf16[224,256]{1,0:T(8,128)(2,1)}, bf16[224,256]{1,0:T(8,128)(2,1)S(1)}, u32[]{:S(2)}, u32[]{:S(2)}) collective-permute-start(bf16[224,256]{1,0:T(8,128)(2,1)} %collective-permute-done.8.refs_8_), channel_id=1, source_target_pairs={{0,8},{2,10},{4,12},{6,14},{8,16},{10,18},{12,20},{14,22},{16,24},... | collective-permute-start | bytes 344072 | tf_op jit(solution)/shard_map/ppermute | solution.py:48
  49.1 1.3 %collective-permute-start.17 = (bf16[224,256]{1,0:T(8,128)(2,1)}, bf16[224,256]{1,0:T(8,128)(2,1)}, u32[]{:S(2)}, u32[]{:S(2)}) collective-permute-start(bf16[224,256]{1,0:T(8,128)(2,1)} %collective-permute-done.8.refs_8_), channel_id=1, source_target_pairs={{0,16},{2,18},{4,20},{6,22},{8,24},{10,26},{12,28},{14,30},{1,17},... | collective-permute-start | bytes 344072 | tf_op jit(solution)/shard_map/ppermute | solution.py:48
  50.4 1.3 %collective-permute-start.18 = (bf16[224,256]{1,0:T(8,128)(2,1)}, bf16[224,256]{1,0:T(8,128)(2,1)}, u32[]{:S(2)}, u32[]{:S(2)}) collective-permute-start(bf16[224,256]{1,0:T(8,128)(2,1)} %collective-permute-done.8.refs_8_), channel_id=1, source_target_pairs={{0,24},{2,26},{4,28},{6,30},{1,25},{3,27},{5,29},{7,31}} | collective-permute-start | bytes 344072 | tf_op jit(solution)/shard_map/ppermute | solution.py:48
  53.6 11.5 %attention_first.1 = (f32[12,256]{1,0:T(8,128)S(1)}, f32[12,80,256]{2,1,0:T(8,128)S(1)}) custom-call(s32[5]{0:T(128)S(1)} %stack.85.vis_ref, bf16[512,384]{1,0:T(8,128)(2,1)S(1)} %copy-done.6, bf16[256,384]{1,0:T(8,128)(2,1)S(1)} %bitcast.33, bf16[256,512]{1,0:T(8,128)(2,1)S(1)} %broadcast_maximum_fusion.2.refs_2_, bf16[512,256]{1,0:T(8,128)(2,1)S(1)} %bitcast.31, ...), custom_call_target="tpu_custom_call" | custom-call | flops 4529848320 | bytes 4194304 | tf_op jit(solution)/shard_map/attention_first/pallas_call | solution.py:388
  66.1 1.5 %convolution_convert_fusion.1 = bf16[384,1024]{1,0:T(8,128)(2,1)} fusion(bf16[384,512]{1,0:T(8,128)(2,1)S(1)} %multiply_convert_fusion, bf16[512,2048]{1,0:T(8,128)(2,1)S(1)} %copy-done, s32[]{:T(128)S(6)} %select_n.29), kind=kOutput, calls=%fused_computation.3 | convolution fusion | flops 403046400 | bytes 2228228 | tf_op jit(solution)/shard_map/dot_general | solution.py:577
  67.6 1.3 %collective-permute-start.26 = (bf16[384,1024]{1,0:T(8,128)(2,1)}, bf16[384,1024]{1,0:T(8,128)(2,1)}, u32[]{:S(2)}, u32[]{:S(2)}) collective-permute-start(bf16[384,1024]{1,0:T(8,128)(2,1)} %convolution_convert_fusion.1), channel_id=1, source_target_pairs={{1,0},{0,1},{3,2},{2,3},{5,4},{4,5},{7,6},{6,7},{9,8},{8,9},{11,10... | collective-permute-start | bytes 2359304 | tf_op jit(solution)/shard_map/ppermute | solution.py:545
  69.6 1.6 %fusion.10 = f32[384,1024]{1,0:T(8,128)S(1)} fusion(bf16[384,512]{1,0:T(8,128)(2,1)} %copy-done.10, bf16[512,2048]{1,0:T(8,128)(2,1)S(1)} %copy-done, s32[]{:T(128)S(6)} %select_n.27), kind=kOutput, calls=%fused_computation.16 | convolution fusion | flops 402653184 | bytes 3014660 | tf_op jit(solution)/shard_map/dot_general | solution.py:577
  72.2 1.4 %convert_add_fusion = f32[384,1024]{1,0:T(8,128)S(1)} fusion(f32[384,1024]{1,0:T(8,128)S(1)} %fusion.10, bf16[384,1024]{1,0:T(8,128)(2,1)} %collective-permute-done.26), kind=kLoop, calls=%fused_computation.1 | loop fusion | flops 786432 | bytes 3932160 | tf_op jit(solution)/shard_map/add | solution.py:583
  73.6 20.2 %attention_rest.1 = bf16[384,512]{1,0:T(8,128)(2,1)S(1)} custom-call(s32[10]{0:T(128)S(1)} %stack.78.vis_ref, bf16[512,384]{1,0:T(8,128)(2,1)S(1)} %copy-done.7, bf16[256,384]{1,0:T(8,128)(2,1)S(1)} %bitcast.34, bf16[256,512]{1,0:T(8,128)(2,1)S(1)} %broadcast_maximum_fusion.2.refs_2_, bf16[512,256]{1,0:T(8,128)(2,1)S(1)} %bitcast.32, ...), custom_call_target="tpu_custom_call" | custom-call | flops 7549747200 | bytes 4194304 | tf_op jit(solution)/shard_map/attention_rest/pallas_call | solution.py:388
  96.9 1.2 %add_convert_fusion = bf16[384,1024]{1,0:T(8,128)(2,1)} fusion(f32[384,1024]{1,0:T(8,128)S(1)} %convert_add_fusion, f32[384,1024]{1,0:T(8,128)S(1)} %fusion.7, bf16[384,1024]{1,0:T(8,128)(2,1)S(1)} %collective-permute-done.27, f32[384]{0:T(512)S(1)} %rsqrt_reduce_fusion), kind=kLoop, calls=%fused_computation | loop fusion | flops 1966080 | bytes 4720128 | tf_op jit(solution)/shard_map/convert_element_type | solution.py:598
  (134 shorter events, 22.6 us)
Async XLA Ops:
  0.0 5.6 %collective-permute-start = (bf16[384,1024]{1,0:T(8,128)(2,1)}, bf16[384,1024]{1,0:T(8,128)(2,1)S(1)}, u32[]{:S(2)}, u32[]{:S(2)}) collective-permute-start(bf16[384,1024]{1,0:T(8,128)(2,1)} %param.18), channel_id=1, source_target_pairs={{1,0},{0,1},{3,2},{2,3},{5,4},{4,5},{7,6},{6,7},{9,8},{8,9},{11,10... | collective-permute-start | bytes 2359304 | tf_op jit(solution)/shard_map/ppermute | solution.py:58
  14.3 5.5 %collective-permute-start.1 = (bf16[32,512]{1,0:T(8,128)(2,1)S(1)}, bf16[32,512]{1,0:T(8,128)(2,1)S(1)}, u32[]{:S(2)}, u32[]{:S(2)}) collective-permute-start(bf16[32,512]{1,0:T(8,128)(2,1)S(1)} %slice.20), channel_id=1, source_target_pairs={{0,2},{2,4},{4,6},{6,8},{8,10},{10,12},{12,14},{14,16},{16,18},{18... | collective-permute-start | bytes 98312 | tf_op jit(solution)/shard_map/ppermute | solution.py:48
  24.8 10.1 %collective-permute-start.8 = (bf16[224,256]{1,0:T(8,128)(2,1)S(1)}, bf16[224,256]{1,0:T(8,128)(2,1)}, u32[]{:S(2)}, u32[]{:S(2)}) collective-permute-start(bf16[224,256]{1,0:T(8,128)(2,1)S(1)} %get-tuple-element.35), channel_id=1, source_target_pairs={{0,6},{2,4},{4,2},{6,0},{8,14},{10,12},{12,10},{14,8},{16,22},{18,... | collective-permute-start | bytes 344072 | tf_op jit(solution)/shard_map/ppermute | solution.py:52
  26.9 7.7 %collective-permute-start.20 = (f32[1,384]{1,0:T(1,128)S(1)}, f32[1,384]{1,0:T(1,128)S(1)}, u32[]{:S(2)}, u32[]{:S(2)}) collective-permute-start(f32[1,384]{1,0:T(1,128)S(1)} %broadcast_in_dim.13), channel_id=1, source_target_pairs={{1,0},{0,1},{3,2},{2,3},{5,4},{4,5},{7,6},{6,7},{9,8},{8,9},{11,10... | collective-permute-start | bytes 4616 | tf_op jit(solution)/shard_map/ppermute | solution.py:58
  28.5 8.5 %collective-permute-start.10 = (bf16[224,256]{1,0:T(8,128)(2,1)S(1)}, bf16[224,256]{1,0:T(8,128)(2,1)S(1)}, u32[]{:S(2)}, u32[]{:S(2)}) collective-permute-start(bf16[224,256]{1,0:T(8,128)(2,1)S(1)} %get-tuple-element.35), channel_id=1, source_target_pairs={{0,8},{2,10},{4,12},{6,14},{8,16},{10,18},{12,20},{14,22},{16,24},... | collective-permute-start | bytes 344072 | tf_op jit(solution)/shard_map/ppermute | solution.py:48
  31.7 7.1 %collective-permute-start.12 = (bf16[224,256]{1,0:T(8,128)(2,1)S(1)}, bf16[224,256]{1,0:T(8,128)(2,1)S(1)}, u32[]{:S(2)}, u32[]{:S(2)}) collective-permute-start(bf16[224,256]{1,0:T(8,128)(2,1)S(1)} %get-tuple-element.35), channel_id=1, source_target_pairs={{0,16},{2,18},{4,20},{6,22},{8,24},{10,26},{12,28},{14,30},{1,17},... | collective-permute-start | bytes 344072 | tf_op jit(solution)/shard_map/ppermute | solution.py:48
  33.0 7.2 %collective-permute-start.4 = (bf16[224,256]{1,0:T(8,128)(2,1)S(1)}, bf16[224,256]{1,0:T(8,128)(2,1)S(1)}, u32[]{:S(2)}, u32[]{:S(2)}) collective-permute-start(bf16[224,256]{1,0:T(8,128)(2,1)S(1)} %get-tuple-element.35), channel_id=1, source_target_pairs={{0,2},{2,0},{4,6},{6,4},{8,10},{10,8},{12,14},{14,12},{16,18},{18,... | collective-permute-start | bytes 344072 | tf_op jit(solution)/shard_map/ppermute | solution.py:52
  34.6 5.5 %collective-permute-start.6 = (bf16[224,256]{1,0:T(8,128)(2,1)S(1)}, bf16[224,256]{1,0:T(8,128)(2,1)S(1)}, u32[]{:S(2)}, u32[]{:S(2)}) collective-permute-start(bf16[224,256]{1,0:T(8,128)(2,1)S(1)} %get-tuple-element.35), channel_id=1, source_target_pairs={{0,4},{2,6},{4,0},{6,2},{8,12},{10,14},{12,8},{14,10},{16,20},{18,... | collective-permute-start | bytes 344072 | tf_op jit(solution)/shard_map/ppermute | solution.py:52
  35.0 5.6 %collective-permute-start.2 = (bf16[224,256]{1,0:T(8,128)(2,1)S(1)}, bf16[224,256]{1,0:T(8,128)(2,1)S(1)}, u32[]{:S(2)}, u32[]{:S(2)}) collective-permute-start(bf16[224,256]{1,0:T(8,128)(2,1)S(1)} %get-tuple-element.35), channel_id=1, source_target_pairs={{0,24},{2,26},{4,28},{6,30},{1,25},{3,27},{5,29},{7,31}} | collective-permute-start | bytes 344072 | tf_op jit(solution)/shard_map/ppermute | solution.py:48
  37.0 3.8 %collective-permute-start.9 = (bf16[224,256]{1,0:T(8,128)(2,1)}, bf16[224,256]{1,0:T(8,128)(2,1)S(1)}, u32[]{:S(2)}, u32[]{:S(2)}) collective-permute-start(bf16[224,256]{1,0:T(8,128)(2,1)} %collective-permute-done.8.refs_8_), channel_id=1, source_target_pairs={{1,0},{0,1},{3,2},{2,3},{5,4},{4,5},{7,6},{6,7},{9,8},{8,9},{11,10... | collective-permute-start | bytes 344072 | tf_op jit(solution)/shard_map/ppermute | solution.py:58
  38.8 3.7 %collective-permute-start.11 = (bf16[224,256]{1,0:T(8,128)(2,1)S(1)}, bf16[224,256]{1,0:T(8,128)(2,1)S(1)}, u32[]{:S(2)}, u32[]{:S(2)}) collective-permute-start(bf16[224,256]{1,0:T(8,128)(2,1)S(1)} %collective-permute-done.10.refs_10_), channel_id=1, source_target_pairs={{1,0},{0,1},{3,2},{2,3},{5,4},{4,5},{7,6},{6,7},{9,8},{8,9},{11,10... | collective-permute-start | bytes 344072 | tf_op jit(solution)/shard_map/ppermute | solution.py:58
  40.1 2.6 %collective-permute-start.13 = (bf16[224,256]{1,0:T(8,128)(2,1)S(1)}, bf16[224,256]{1,0:T(8,128)(2,1)S(1)}, u32[]{:S(2)}, u32[]{:S(2)}) collective-permute-start(bf16[224,256]{1,0:T(8,128)(2,1)S(1)} %collective-permute-done.12.refs_12_), channel_id=1, source_target_pairs={{1,0},{0,1},{3,2},{2,3},{5,4},{4,5},{7,6},{6,7},{9,8},{8,9},{11,10... | collective-permute-start | bytes 344072 | tf_op jit(solution)/shard_map/ppermute | solution.py:58
  40.1 8.9 %collective-permute-start.5 = (bf16[224,256]{1,0:T(8,128)(2,1)S(1)}, bf16[224,256]{1,0:T(8,128)(2,1)S(1)}, u32[]{:S(2)}, u32[]{:S(2)}) collective-permute-start(bf16[224,256]{1,0:T(8,128)(2,1)S(1)} %collective-permute-done.4.refs_4_), channel_id=1, source_target_pairs={{1,0},{0,1},{3,2},{2,3},{5,4},{4,5},{7,6},{6,7},{9,8},{8,9},{11,10... | collective-permute-start | bytes 344072 | tf_op jit(solution)/shard_map/ppermute | solution.py:58
  40.7 9.7 %collective-permute-start.7 = (bf16[224,256]{1,0:T(8,128)(2,1)S(1)}, bf16[224,256]{1,0:T(8,128)(2,1)S(1)}, u32[]{:S(2)}, u32[]{:S(2)}) collective-permute-start(bf16[224,256]{1,0:T(8,128)(2,1)S(1)} %collective-permute-done.6.refs_6_), channel_id=1, source_target_pairs={{1,0},{0,1},{3,2},{2,3},{5,4},{4,5},{7,6},{6,7},{9,8},{8,9},{11,10... | collective-permute-start | bytes 344072 | tf_op jit(solution)/shard_map/ppermute | solution.py:58
  40.8 25.3 %collective-permute-start.14 = (bf16[3,224,256]{2,1,0:T(8,128)(2,1)S(1)}, bf16[3,224,256]{2,1,0:T(8,128)(2,1)}, u32[]{:S(2)}, u32[]{:S(2)}) collective-permute-start(bf16[3,224,256]{2,1,0:T(8,128)(2,1)S(1)} %pad_maximum_fusion), channel_id=1, source_target_pairs={{0,2},{2,0},{4,6},{6,4},{8,10},{10,8},{12,14},{14,12},{16,18},{18,... | collective-permute-start | bytes 1032200 | tf_op jit(solution)/shard_map/ppermute | solution.py:52
  42.5 23.6 %collective-permute-start.15 = (bf16[3,224,256]{2,1,0:T(8,128)(2,1)S(1)}, bf16[3,224,256]{2,1,0:T(8,128)(2,1)}, u32[]{:S(2)}, u32[]{:S(2)}) collective-permute-start(bf16[3,224,256]{2,1,0:T(8,128)(2,1)S(1)} %pad_maximum_fusion), channel_id=1, source_target_pairs={{0,4},{2,6},{4,0},{6,2},{8,12},{10,14},{12,8},{14,10},{16,20},{18,... | collective-permute-start | bytes 1032200 | tf_op jit(solution)/shard_map/ppermute | solution.py:52
  42.8 23.3 %collective-permute-start.16 = (bf16[224,256]{1,0:T(8,128)(2,1)}, bf16[224,256]{1,0:T(8,128)(2,1)S(1)}, u32[]{:S(2)}, u32[]{:S(2)}) collective-permute-start(bf16[224,256]{1,0:T(8,128)(2,1)} %collective-permute-done.8.refs_8_), channel_id=1, source_target_pairs={{0,8},{2,10},{4,12},{6,14},{8,16},{10,18},{12,20},{14,22},{16,24},... | collective-permute-start | bytes 344072 | tf_op jit(solution)/shard_map/ppermute | solution.py:48
  49.1 17.0 %collective-permute-start.17 = (bf16[224,256]{1,0:T(8,128)(2,1)}, bf16[224,256]{1,0:T(8,128)(2,1)}, u32[]{:S(2)}, u32[]{:S(2)}) collective-permute-start(bf16[224,256]{1,0:T(8,128)(2,1)} %collective-permute-done.8.refs_8_), channel_id=1, source_target_pairs={{0,16},{2,18},{4,20},{6,22},{8,24},{10,26},{12,28},{14,30},{1,17},... | collective-permute-start | bytes 344072 | tf_op jit(solution)/shard_map/ppermute | solution.py:48
  50.4 15.7 %collective-permute-start.18 = (bf16[224,256]{1,0:T(8,128)(2,1)}, bf16[224,256]{1,0:T(8,128)(2,1)}, u32[]{:S(2)}, u32[]{:S(2)}) collective-permute-start(bf16[224,256]{1,0:T(8,128)(2,1)} %collective-permute-done.8.refs_8_), channel_id=1, source_target_pairs={{0,24},{2,26},{4,28},{6,30},{1,25},{3,27},{5,29},{7,31}} | collective-permute-start | bytes 344072 | tf_op jit(solution)/shard_map/ppermute | solution.py:48
  67.6 4.1 %collective-permute-start.26 = (bf16[384,1024]{1,0:T(8,128)(2,1)}, bf16[384,1024]{1,0:T(8,128)(2,1)}, u32[]{:S(2)}, u32[]{:S(2)}) collective-permute-start(bf16[384,1024]{1,0:T(8,128)(2,1)} %convolution_convert_fusion.1), channel_id=1, source_target_pairs={{1,0},{0,1},{3,2},{2,3},{5,4},{4,5},{7,6},{6,7},{9,8},{8,9},{11,10... | collective-permute-start | bytes 2359304 | tf_op jit(solution)/shard_map/ppermute | solution.py:545
  68.9 2.7 %collective-permute-start.3 = (bf16[224,256]{1,0:T(8,128)(2,1)S(1)}, bf16[224,256]{1,0:T(8,128)(2,1)S(1)}, u32[]{:S(2)}, u32[]{:S(2)}) collective-permute-start(bf16[224,256]{1,0:T(8,128)(2,1)S(1)} %collective-permute-done.2.refs_4_), channel_id=1, source_target_pairs={{1,0},{0,1},{3,2},{2,3},{5,4},{4,5},{7,6},{6,7},{9,8},{8,9},{11,10... | collective-permute-start | bytes 344072 | tf_op jit(solution)/shard_map/ppermute | solution.py:58
  69.0 4.6 %collective-permute-start.21 = (bf16[3,224,256]{2,1,0:T(8,128)(2,1)}, bf16[3,224,256]{2,1,0:T(8,128)(2,1)S(1)}, u32[]{:S(2)}, u32[]{:S(2)}) collective-permute-start(bf16[3,224,256]{2,1,0:T(8,128)(2,1)} %collective-permute-done.14.refs_6_), channel_id=1, source_target_pairs={{1,0},{0,1},{3,2},{2,3},{5,4},{4,5},{7,6},{6,7},{9,8},{8,9},{11,10... | collective-permute-start | bytes 1032200 | tf_op jit(solution)/shard_map/ppermute | solution.py:58
  69.5 4.1 %collective-permute-start.22 = (bf16[3,224,256]{2,1,0:T(8,128)(2,1)}, bf16[3,224,256]{2,1,0:T(8,128)(2,1)S(1)}, u32[]{:S(2)}, u32[]{:S(2)}) collective-permute-start(bf16[3,224,256]{2,1,0:T(8,128)(2,1)} %collective-permute-done.15.refs_8_), channel_id=1, source_target_pairs={{1,0},{0,1},{3,2},{2,3},{5,4},{4,5},{7,6},{6,7},{9,8},{8,9},{11,10... | collective-permute-start | bytes 1032200 | tf_op jit(solution)/shard_map/ppermute | solution.py:58
  71.2 2.4 %collective-permute-start.23 = (bf16[224,256]{1,0:T(8,128)(2,1)S(1)}, bf16[224,256]{1,0:T(8,128)(2,1)S(1)}, u32[]{:S(2)}, u32[]{:S(2)}) collective-permute-start(bf16[224,256]{1,0:T(8,128)(2,1)S(1)} %collective-permute-done.16.refs_10_), channel_id=1, source_target_pairs={{1,0},{0,1},{3,2},{2,3},{5,4},{4,5},{7,6},{6,7},{9,8},{8,9},{11,10... | collective-permute-start | bytes 344072 | tf_op jit(solution)/shard_map/ppermute | solution.py:58
  (31 other events, 231.6 us)

commit v2 on v1

--- a/solution.py
+++ b/solution.py
@@ -158,7 +158,7 @@
     return width, out
 
 
-def attention_kernel(first, last, counts, rows, groups, heads, vis_ref, *refs):
+def attention_kernel(first, last, counts, order, rows, groups, heads, vis_ref, *refs):
     refs = list(refs)
     qt_ref, qrt_ref, key_up_ref, value_up_ref = refs[:4]
     refs = refs[4:]
@@ -216,21 +216,20 @@
     at = 1 if first else 0
     slot = 0
     is_bias = lax.broadcasted_iota(jnp.int32, (queries, 128), 1) == ROT_DIM
-    for source, several in zip(sources, counts):
-        for index in range(several[0] or 1):
-            rots = []
-            base = (at % 2) * queries
-            for n, ref in enumerate(source):
-                view = ref.at[index] if several[0] else ref
-                lat_ref[at // 2, base + n * rows : base + (n + 1) * rows, :] = view[:rows, :]
-                packed = view[rows:, :].astype(jnp.float32)[: rows // groups]
-                rots += [packed[:, g * ROT_DIM : (g + 1) * ROT_DIM] for g in range(groups)]
-            rot = jnp.concatenate(rots, axis=0)
-            rot = jnp.concatenate([rot, jnp.zeros((queries, 128 - ROT_DIM), jnp.float32)], axis=1)
-            bias = jnp.where(vis_ref[slot] > 0, 0.0, far_below)
-            rot_ref[at // 2, base : base + queries, :] = jnp.where(is_bias, bias, rot).astype(jnp.bfloat16)
-            at += 1
-            slot += 1
+    for place, index in order:
+        rots = []
+        base = (at % 2) * queries
+        for n, ref in enumerate(sources[place]):
+            view = ref.at[index] if counts[place][0] else ref
+            lat_ref[at // 2, base + n * rows : base + (n + 1) * rows, :] = view[:rows, :]
+            packed = view[rows:, :].astype(jnp.float32)[: rows // groups]
+            rots += [packed[:, g * ROT_DIM : (g + 1) * ROT_DIM] for g in range(groups)]
+        rot = jnp.concatenate(rots, axis=0)
+        rot = jnp.concatenate([rot, jnp.zeros((queries, 128 - ROT_DIM), jnp.float32)], axis=1)
+        bias = jnp.where(vis_ref[slot] > 0, 0.0, far_below)
+        rot_ref[at // 2, base : base + queries, :] = jnp.where(is_bias, bias, rot).astype(jnp.bfloat16)
+        at += 1
+        slot += 1
     if at % 2:
         lat_ref[at // 2, queries:, :] = jnp.zeros((queries, lat_ref.shape[2]), jnp.bfloat16)
         rot_ref[at // 2, queries:, :] = jnp.where(is_bias, far_below, 0.0).astype(jnp.bfloat16)
@@ -348,7 +347,7 @@
 
 
 def attention_stage(visible, queries_t, query_rot_t, key_up, value_up, slots, rows, groups,
-                    own=None, state=None, last=False):
+                    order, own=None, state=None, last=False):
     first = own is not None
     heads = key_up.shape[1] // NOPE_DIM
     tok_rows = queries_t.shape[1]
@@ -386,7 +385,7 @@
     flops = 2 * total_blocks * tok_rows * tok_rows * heads * (256 + VALUE_DIM)
     in_vmem = pl.BlockSpec()
     return pl.pallas_call(
-        functools.partial(attention_kernel, first, last, counts, rows, groups, heads),
+        functools.partial(attention_kernel, first, last, counts, order, rows, groups, heads),
         in_specs=[pl.BlockSpec(memory_space=pltpu.SMEM)] + [in_vmem] * (len(consts) + len(flat) + len(extra)),
         out_specs=in_vmem if last else (in_vmem, in_vmem),
         scratch_shapes=scratch,
@@ -489,12 +488,9 @@
     plane = 4 if sp_size % 4 == 0 else 1
     high, low = sp_index // plane, sp_index % plane
     far = range(1, sp_size // plane)
-    near, column = [], []
-    for b in range(1, plane):
-        near.append(swap_bits(mine, "sp", b))
+    column = []
     for s in far:
         column.append(shift_by(mine, "sp", plane * s))
-    near_vis = [((low ^ b) < low).astype(jnp.int32) for b in range(1, plane)]
     column_vis = [(high >= s).astype(jnp.int32) for s in far]
 
     def with_pieces(arrays):
@@ -557,22 +553,21 @@
         rows=rows,
         groups=groups,
     )
-    slots_one, vis_one = with_pieces(near + column), near_vis + column_vis
-    slots_two, vis_two = [], []
+    state = None
+    arrived, vis_rest, order_rest = [], [], []
+    slots, vis, order = with_pieces(column), column_vis, [(n, 0) for n in range(len(column))]
     if plane == 4:
-        if len(slots_one) % 2 == 0:
-            slots_two, vis_two = slots_one[-1:], vis_one[-1:]
-            slots_one, vis_one = slots_one[:-1], vis_one[:-1]
-        column_all = jnp.stack(column)
-        arrived = []
-        for b in (1, 2):
+        column_all = jnp.stack([mine] + column)
+        for b in range(1, plane):
             arrived.append(swap_bits(column_all, "sp", b))
-        for s in far:
-            arrived.append(shift_by(near[2], "sp", plane * s))
-        state = stage(jnp.stack(vis_one), slots=slots_one, own=own)
-        state, arrived, conv_mixed = lax.optimization_barrier((state, arrived, conv_mixed))
-        slots_two = slots_two + with_pieces(arrived)
-        vis_two = vis_two + column_vis * 3
+        for s in range(len(column) + 1):
+            for b in range(1, plane):
+                order_rest.append((b - 1, s))
+                vis_rest.append(column_vis[s - 1] if s else ((low ^ b) < low).astype(jnp.int32))
+        if slots:
+            state = stage(jnp.stack(vis), slots=slots, order=order, own=own)
+            state, arrived, conv_mixed = lax.optimization_barrier((state, arrived, conv_mixed))
+        slots, vis, order = with_pieces(arrived), vis_rest, order_rest
     conv_own, conv_rest = scatter(
         lambda device: jnp.dot(
             conv_mixed, columns_of(device, conv_out_weight), preferred_element_type=f32
@@ -581,11 +576,11 @@
     conv_part = conv_own
     for part in conv_rest:
         conv_part = conv_part + part.astype(f32)
-    if slots_two:
+    if state is not None:
         state, conv_part = lax.optimization_barrier((state, conv_part))
-        attended = stage(jnp.stack(vis_two), slots=slots_two, state=state, last=True)
+        attended = stage(jnp.stack(vis), slots=slots, order=order, state=state, last=True)
     else:
-        attended = stage(jnp.stack(vis_one), slots=slots_one, own=own, last=True)
+        attended = stage(jnp.stack(vis), slots=slots, order=order, own=own, last=True)
 
     wide_att = attended.astype(f32)
     att_sq = total(jnp.sum(wide_att * wide_att, axis=1)[None, :], "tp")[0]

time: 98.7 us -> 97.7 us (0.990)
  the two profiles are of different devices: /device:TPU:21 before, /device:TPU:31 now
where the time goes in v2:
time: 97.7 us; the launch traced here: 96.1 us
  Pallas kernels  37.5 us (38%)
  starting transfers between devices  16.1 us (16%)
  waiting for transfers between devices  15.1 us (15%)
  other arithmetic  10.9 us (11%)
  matrix products  9.1 us (9%)
  local copies, waits for them, and re-layouts  6.87 us (7%)
    pallas_call x2, Pallas kernels, attention_stage(): pl.pallas_call(functools.partial(attention_kernel, first, last, counts, o...  32.1 us
    ppermute x4, waiting for transfers between devices, shift_by(): lax.ppermute(block, axis, [(i, i + distance) for i in devices if i + dist...  8.19 us
    ppermute x10, starting transfers between devices, others(): lax.ppermute(block, axis, [((i + d) % size, i) for i in range(size)])  7.13 us
    unnamed x53, local copies, waits for them, and re-layouts  6.51 us
    ppermute x3, waiting for transfers between devices, swap_bits(): lax.ppermute(block, axis, [(i, i ^ bits) for i in range(lax.axis_size(axi...  5.5 us
    ppermute x4, starting transfers between devices, shift_by(): lax.ppermute(block, axis, [(i, i + distance) for i in devices if i + dist...  5.34 us
    dot_general x4, matrix products, project(): return jnp.dot(scaled, weight, preferred_element_type=f32)  4.9 us
    max x6, other arithmetic, near_by(): return jnp.maximum(array, jnp.finfo(array.dtype).min)  3.71 us
  transfers between devices with their start and end apart: 19, of which 7 were waited for; matrix products, arithmetic and copies ran while one was open for 13% of the time, Pallas kernels for 9%

profile of v2, /device:TPU:31, one launch (start us, length us, event | category | flops | bytes accessed | tf_op | source)
XLA Modules:
  0.0 96.1 jit_solution(11730062874476438300)
XLA Ops:
  3.5 1.3 %broadcast_maximum_fusion.1.refs_0_ = bf16[384,1024]{1,0:T(8,128)(2,1)S(1)} fusion(bf16[384,1024]{1,0:T(8,128)(2,1)} %param.18), kind=kLoop, calls=%fused_computation.30 | loop fusion | flops 393216 | bytes 1572864 | tf_op jit(solution)/shard_map/max | solution.py:471
  5.1 2.0 %front.1 = (bf16[384,2048]{1,0:T(8,128)(2,1)S(1)}, f32[384,1]{1,0:T(8,128)S(1)}, bf16[384,256]{1,0:T(8,128)(2,1)S(1)}, bf16[384,128]{1,0:T(8,128)(2,1)S(1)}, bf16[224,256]{1,0:T(8,128)(2,1)S(1)}) custom-call(s32[1]{0:T(128)} %bitcast.6.index_ref, bf16[384,1024]{1,0:T(8,128)(2,1)S(1)} %broadcast_maximum_fusion.1.refs_0_, ...), custom_call_target="tpu_custom_call" | custom-call | flops 805306368 | bytes 8388608 | tf_op jit(solution)/shard_map/front/pallas_call | solution.py:127
  11.8 2.0 %fusion.14.refs_0_ = bf16[512,384]{1,0:T(8,128)(2,1)} fusion(f32[384]{0:T(512)S(1)} %get-tuple-element.51, bf16[384,2048]{1,0:T(8,128)(2,1)S(1)} %get-tuple-element.30, bf16[2048,512]{1,0:T(8,128)(2,1)S(1)} %copy-done.25), kind=kOutput, calls=%fused_computation.29 | convolution fusion | flops 805699584 | bytes 4064768 | tf_op jit(solution)/shard_map/dot_general | solution.py:500
  13.8 1.3 %collective-permute-start.1 = (bf16[32,512]{1,0:T(8,128)(2,1)S(1)}, bf16[32,512]{1,0:T(8,128)(2,1)S(1)}, u32[]{:S(2)}, u32[]{:S(2)}) collective-permute-start(bf16[32,512]{1,0:T(8,128)(2,1)S(1)} %slice.20), channel_id=1, source_target_pairs={{0,2},{2,4},{4,6},{6,8},{8,10},{10,12},{12,14},{14,16},{16,18},{18... | collective-permute-start | bytes 98312 | tf_op jit(solution)/shard_map/ppermute | solution.py:48
  15.1 3.3 %collective-permute-done.1.rim_ref = bf16[32,512]{1,0:T(8,128)(2,1)S(1)} collective-permute-done((bf16[32,512]{1,0:T(8,128)(2,1)S(1)}, bf16[32,512]{1,0:T(8,128)(2,1)S(1)}, u32[]{:S(2)}, u32[]{:S(2)}) %collective-permute-start.1) | collective-permute-done | bytes 32800 | tf_op jit(solution)/shard_map/ppermute | solution.py:48
  18.5 3.3 %conv.1 = f32[384,512]{1,0:T(8,128)S(1)} custom-call(bf16[384,512]{1,0:T(8,128)(2,1)S(1)} %fusion.5.gated_ref, bf16[32,512]{1,0:T(8,128)(2,1)S(1)} %collective-permute-done.1.rim_ref, f32[31,512]{1,0:T(8,128)S(1)} %copy-done.5), custom_call_target="tpu_custom_call" | custom-call | flops 609484800 | bytes 1179648 | tf_op jit(solution)/shard_map/conv/pallas_call | solution.py:423
  22.0 1.4 %collective-permute-start.11 = (f32[2,384]{1,0:T(2,128)S(1)}, f32[2,384]{1,0:T(2,128)S(1)}, u32[]{:S(2)}, u32[]{:S(2)}) collective-permute-start(f32[2,384]{1,0:T(2,128)S(1)} %pad_maximum_fusion.4), channel_id=1, source_target_pairs={{1,0},{0,1},{3,2},{2,3},{5,4},{4,5},{7,6},{6,7},{9,8},{8,9},{11,10... | collective-permute-start | bytes 9224 | tf_op jit(solution)/shard_map/ppermute | solution.py:58
  23.4 1.3 %collective-permute-start.2 = (bf16[224,256]{1,0:T(8,128)(2,1)S(1)}, bf16[224,256]{1,0:T(8,128)(2,1)}, u32[]{:S(2)}, u32[]{:S(2)}) collective-permute-start(bf16[224,256]{1,0:T(8,128)(2,1)S(1)} %get-tuple-element.33), channel_id=1, source_target_pairs={{0,8},{2,10},{4,12},{6,14},{8,16},{10,18},{12,20},{14,22},{16,24},... | collective-permute-start | bytes 344072 | tf_op jit(solution)/shard_map/ppermute | solution.py:48
  24.7 1.3 %collective-permute-start.4 = (bf16[224,256]{1,0:T(8,128)(2,1)S(1)}, bf16[224,256]{1,0:T(8,128)(2,1)}, u32[]{:S(2)}, u32[]{:S(2)}) collective-permute-start(bf16[224,256]{1,0:T(8,128)(2,1)S(1)} %get-tuple-element.33), channel_id=1, source_target_pairs={{0,16},{2,18},{4,20},{6,22},{8,24},{10,26},{12,28},{14,30},{1,17},... | collective-permute-start | bytes 344072 | tf_op jit(solution)/shard_map/ppermute | solution.py:48
  26.0 1.5 %collective-permute-start.6 = (bf16[224,256]{1,0:T(8,128)(2,1)S(1)}, bf16[224,256]{1,0:T(8,128)(2,1)}, u32[]{:S(2)}, u32[]{:S(2)}) collective-permute-start(bf16[224,256]{1,0:T(8,128)(2,1)S(1)} %get-tuple-element.33), channel_id=1, source_target_pairs={{0,24},{2,26},{4,28},{6,30},{1,25},{3,27},{5,29},{7,31}} | collective-permute-start | bytes 344072 | tf_op jit(solution)/shard_map/ppermute | solution.py:48
  27.6 1.3 %multiply_reduce_fusion = (f32[384]{0:T(512)S(1)}, f32[384,512]{1,0:T(8,128)}) fusion(f32[512]{0:T(512)S(1)} %copy-done.19, f32[512]{0:T(512)S(1)} %copy-done.20, f32[384]{0:T(512)S(1)} %add_rsqrt_fusion, f32[384,512]{1,0:T(8,128)S(1)} %conv.1, f32[384]{0:T(512)S(1)} %get-tuple-element.53), kind=kLoop, calls=%fused_computation.23 | loop fusion | flops 1965696 | bytes 1581568 | tf_op jit(solution)/shard_map/reduce_sum | solution.py:527
  30.1 2.6 %collective-permute-start.3 = (bf16[224,256]{1,0:T(8,128)(2,1)}, bf16[224,256]{1,0:T(8,128)(2,1)S(1)}, u32[]{:S(2)}, u32[]{:S(2)}) collective-permute-start(bf16[224,256]{1,0:T(8,128)(2,1)} %collective-permute-done.2.refs_4_), channel_id=1, source_target_pairs={{1,0},{0,1},{3,2},{2,3},{5,4},{4,5},{7,6},{6,7},{9,8},{8,9},{11,10... | collective-permute-start | bytes 344072 | tf_op jit(solution)/shard_map/ppermute | solution.py:58
  32.7 4.9 %collective-permute-done.4.refs_6_ = bf16[224,256]{1,0:T(8,128)(2,1)} collective-permute-done((bf16[224,256]{1,0:T(8,128)(2,1)S(1)}, bf16[224,256]{1,0:T(8,128)(2,1)}, u32[]{:S(2)}, u32[]{:S(2)}) %collective-permute-start.4) | collective-permute-done | bytes 114720 | tf_op jit(solution)/shard_map/ppermute | solution.py:48
  38.6 2.0 %collective-permute-start.10 = (bf16[4,224,256]{2,1,0:T(8,128)(2,1)S(1)}, bf16[4,224,256]{2,1,0:T(8,128)(2,1)S(1)}, u32[]{:S(2)}, u32[]{:S(2)}) collective-permute-start(bf16[4,224,256]{2,1,0:T(8,128)(2,1)S(1)} %pad_maximum_fusion), channel_id=1, source_target_pairs={{0,6},{2,4},{4,2},{6,0},{8,14},{10,12},{12,10},{14,8},{16,22},{18,... | collective-permute-start | bytes 1376264 | tf_op jit(solution)/shard_map/ppermute | solution.py:52
  41.3 1.6 %collective-permute-start.5 = (bf16[224,256]{1,0:T(8,128)(2,1)}, bf16[224,256]{1,0:T(8,128)(2,1)S(1)}, u32[]{:S(2)}, u32[]{:S(2)}) collective-permute-start(bf16[224,256]{1,0:T(8,128)(2,1)} %collective-permute-done.4.refs_6_), channel_id=1, source_target_pairs={{1,0},{0,1},{3,2},{2,3},{5,4},{4,5},{7,6},{6,7},{9,8},{8,9},{11,10... | collective-permute-start | bytes 344072 | tf_op jit(solution)/shard_map/ppermute | solution.py:58
  42.9 1.3 %multiply_convert_fusion = bf16[384,512]{1,0:T(8,128)(2,1)S(1)} fusion(f32[384,512]{1,0:T(8,128)} %get-tuple-element.56, f32[512]{0:T(512)S(1)} %copy-done.21, f32[384]{0:T(512)S(1)} %rsqrt_reduce_fusion.1), kind=kLoop, calls=%fused_computation.22 | loop fusion | flops 589824 | bytes 1183232 | tf_op jit(solution)/shard_map/convert_element_type | solution.py:530
  47.3 8.2 %attention_first.1 = (f32[12,256]{1,0:T(8,128)S(1)}, f32[12,80,256]{2,1,0:T(8,128)S(1)}) custom-call(s32[3]{0:T(128)S(1)} %pad_add_fusion.vis_ref, bf16[512,384]{1,0:T(8,128)(2,1)S(1)} %copy-done.6, bf16[256,384]{1,0:T(8,128)(2,1)S(1)} %bitcast.34, bf16[256,512]{1,0:T(8,128)(2,1)S(1)} %broadcast_maximum_fusion.2.refs_2_, bf16[512,256]{1,0:T(8,128)(2,1)S(1)} %bitcast.32, ...), custom_call_target="tpu_custom_call" | custom-call | flops 3019898880 | bytes 4194304 | tf_op jit(solution)/shard_map/attention_first/pallas_call | solution.py:387
  56.5 3.5 %collective-permute-done.8.refs_4_ = bf16[4,224,256]{2,1,0:T(8,128)(2,1)} collective-permute-done((bf16[4,224,256]{2,1,0:T(8,128)(2,1)S(1)}, bf16[4,224,256]{2,1,0:T(8,128)(2,1)}, u32[]{:S(2)}, u32[]{:S(2)}) %collective-permute-start.8) | collective-permute-done | bytes 458784 | tf_op jit(solution)/shard_map/ppermute | solution.py:52
  59.9 2.0 %collective-permute-done.9.refs_6_ = bf16[4,224,256]{2,1,0:T(8,128)(2,1)} collective-permute-done((bf16[4,224,256]{2,1,0:T(8,128)(2,1)S(1)}, bf16[4,224,256]{2,1,0:T(8,128)(2,1)}, u32[]{:S(2)}, u32[]{:S(2)}) %collective-permute-start.9) | collective-permute-done | bytes 458784 | tf_op jit(solution)/shard_map/ppermute | solution.py:52
  62.0 1.5 %convolution_convert_fusion.1 = bf16[384,1024]{1,0:T(8,128)(2,1)} fusion(bf16[384,512]{1,0:T(8,128)(2,1)S(1)} %multiply_convert_fusion, bf16[512,2048]{1,0:T(8,128)(2,1)S(1)} %copy-done, s32[]{:T(128)S(6)} %select_n.29), kind=kOutput, calls=%fused_computation.3 | convolution fusion | flops 403046400 | bytes 2228228 | tf_op jit(solution)/shard_map/dot_general | solution.py:572
  64.7 1.6 %fusion.10 = f32[384,1024]{1,0:T(8,128)S(1)} fusion(bf16[384,512]{1,0:T(8,128)(2,1)} %copy-done.10, bf16[512,2048]{1,0:T(8,128)(2,1)S(1)} %copy-done, s32[]{:T(128)S(6)} %select_n.27), kind=kOutput, calls=%fused_computation.16 | convolution fusion | flops 402653184 | bytes 3014660 | tf_op jit(solution)/shard_map/dot_general | solution.py:572
  66.3 1.5 %convert_add_fusion = f32[384,1024]{1,0:T(8,128)S(1)} fusion(f32[384,1024]{1,0:T(8,128)S(1)} %fusion.10, bf16[384,1024]{1,0:T(8,128)(2,1)} %collective-permute-done.16), kind=kLoop, calls=%fused_computation.1 | loop fusion | flops 786432 | bytes 3932160 | tf_op jit(solution)/shard_map/add | solution.py:578
  68.0 23.9 %attention_rest.1 = bf16[384,512]{1,0:T(8,128)(2,1)S(1)} custom-call(s32[12]{0:T(128)S(1)} %stack.87.vis_ref, bf16[512,384]{1,0:T(8,128)(2,1)S(1)} %copy-done.7, bf16[256,384]{1,0:T(8,128)(2,1)S(1)} %bitcast.35, bf16[256,512]{1,0:T(8,128)(2,1)S(1)} %broadcast_maximum_fusion.2.refs_2_, bf16[512,256]{1,0:T(8,128)(2,1)S(1)} %bitcast.33, ...), custom_call_target="tpu_custom_call" | custom-call | flops 9059696640 | bytes 4194304 | tf_op jit(solution)/shard_map/attention_rest/pallas_call | solution.py:387
  95.0 1.2 %add_convert_fusion = bf16[384,1024]{1,0:T(8,128)(2,1)} fusion(f32[384,1024]{1,0:T(8,128)S(1)} %convert_add_fusion, f32[384,1024]{1,0:T(8,128)S(1)} %fusion.7, bf16[384,1024]{1,0:T(8,128)(2,1)S(1)} %collective-permute-done.17, f32[384]{0:T(512)S(1)} %rsqrt_reduce_fusion), kind=kLoop, calls=%fused_computation | loop fusion | flops 1966080 | bytes 4720128 | tf_op jit(solution)/shard_map/convert_element_type | solution.py:593
  (114 shorter events, 19.9 us)
Async XLA Ops:
  0.0 62.0 %copy-start = (bf16[512,2048]{1,0:T(8,128)(2,1)S(1)}, bf16[512,2048]{1,0:T(8,128)(2,1)}, u32[]{:S(2)}) copy-start(bf16[512,2048]{1,0:T(8,128)(2,1)} %param.35) | copy-start | bytes 6291460
  0.0 5.1 %collective-permute-start = (bf16[384,1024]{1,0:T(8,128)(2,1)}, bf16[384,1024]{1,0:T(8,128)(2,1)S(1)}, u32[]{:S(2)}, u32[]{:S(2)}) collective-permute-start(bf16[384,1024]{1,0:T(8,128)(2,1)} %param.18), channel_id=1, source_target_pairs={{1,0},{0,1},{3,2},{2,3},{5,4},{4,5},{7,6},{6,7},{9,8},{8,9},{11,10... | collective-permute-start | bytes 2359304 | tf_op jit(solution)/shard_map/ppermute | solution.py:58
  13.8 4.6 %collective-permute-start.1 = (bf16[32,512]{1,0:T(8,128)(2,1)S(1)}, bf16[32,512]{1,0:T(8,128)(2,1)S(1)}, u32[]{:S(2)}, u32[]{:S(2)}) collective-permute-start(bf16[32,512]{1,0:T(8,128)(2,1)S(1)} %slice.20), channel_id=1, source_target_pairs={{0,2},{2,4},{4,6},{6,8},{8,10},{10,12},{12,14},{14,16},{16,18},{18... | collective-permute-start | bytes 98312 | tf_op jit(solution)/shard_map/ppermute | solution.py:48
  22.0 5.5 %collective-permute-start.11 = (f32[2,384]{1,0:T(2,128)S(1)}, f32[2,384]{1,0:T(2,128)S(1)}, u32[]{:S(2)}, u32[]{:S(2)}) collective-permute-start(f32[2,384]{1,0:T(2,128)S(1)} %pad_maximum_fusion.4), channel_id=1, source_target_pairs={{1,0},{0,1},{3,2},{2,3},{5,4},{4,5},{7,6},{6,7},{9,8},{8,9},{11,10... | collective-permute-start | bytes 9224 | tf_op jit(solution)/shard_map/ppermute | solution.py:58
  23.4 19.5 %copy-start.21 = (f32[512]{0:T(512)S(1)}, f32[512]{0:T(512)}, u32[]{:S(2)}) copy-start(f32[512]{0:T(512)} %param.33) | copy-start | bytes 6148
  23.4 6.7 %collective-permute-start.2 = (bf16[224,256]{1,0:T(8,128)(2,1)S(1)}, bf16[224,256]{1,0:T(8,128)(2,1)}, u32[]{:S(2)}, u32[]{:S(2)}) collective-permute-start(bf16[224,256]{1,0:T(8,128)(2,1)S(1)} %get-tuple-element.33), channel_id=1, source_target_pairs={{0,8},{2,10},{4,12},{6,14},{8,16},{10,18},{12,20},{14,22},{16,24},... | collective-permute-start | bytes 344072 | tf_op jit(solution)/shard_map/ppermute | solution.py:48
  24.7 12.8 %collective-permute-start.4 = (bf16[224,256]{1,0:T(8,128)(2,1)S(1)}, bf16[224,256]{1,0:T(8,128)(2,1)}, u32[]{:S(2)}, u32[]{:S(2)}) collective-permute-start(bf16[224,256]{1,0:T(8,128)(2,1)S(1)} %get-tuple-element.33), channel_id=1, source_target_pairs={{0,16},{2,18},{4,20},{6,22},{8,24},{10,26},{12,28},{14,30},{1,17},... | collective-permute-start | bytes 344072 | tf_op jit(solution)/shard_map/ppermute | solution.py:48
  26.0 11.5 %collective-permute-start.6 = (bf16[224,256]{1,0:T(8,128)(2,1)S(1)}, bf16[224,256]{1,0:T(8,128)(2,1)}, u32[]{:S(2)}, u32[]{:S(2)}) collective-permute-start(bf16[224,256]{1,0:T(8,128)(2,1)S(1)} %get-tuple-element.33), channel_id=1, source_target_pairs={{0,24},{2,26},{4,28},{6,30},{1,25},{3,27},{5,29},{7,31}} | collective-permute-start | bytes 344072 | tf_op jit(solution)/shard_map/ppermute | solution.py:48
  28.8 1.2 %collective-permute-start.12 = (f32[1,384]{1,0:T(1,128)S(1)}, f32[1,384]{1,0:T(1,128)S(1)}, u32[]{:S(2)}, u32[]{:S(2)}) collective-permute-start(f32[1,384]{1,0:T(1,128)S(1)} %broadcast_in_dim.13), channel_id=1, source_target_pairs={{1,0},{0,1},{3,2},{2,3},{5,4},{4,5},{7,6},{6,7},{9,8},{8,9},{11,10... | collective-permute-start | bytes 4616 | tf_op jit(solution)/shard_map/ppermute | solution.py:58
  30.1 12.8 %collective-permute-start.3 = (bf16[224,256]{1,0:T(8,128)(2,1)}, bf16[224,256]{1,0:T(8,128)(2,1)S(1)}, u32[]{:S(2)}, u32[]{:S(2)}) collective-permute-start(bf16[224,256]{1,0:T(8,128)(2,1)} %collective-permute-done.2.refs_4_), channel_id=1, source_target_pairs={{1,0},{0,1},{3,2},{2,3},{5,4},{4,5},{7,6},{6,7},{9,8},{8,9},{11,10... | collective-permute-start | bytes 344072 | tf_op jit(solution)/shard_map/ppermute | solution.py:58
  38.6 17.8 %collective-permute-start.10 = (bf16[4,224,256]{2,1,0:T(8,128)(2,1)S(1)}, bf16[4,224,256]{2,1,0:T(8,128)(2,1)S(1)}, u32[]{:S(2)}, u32[]{:S(2)}) collective-permute-start(bf16[4,224,256]{2,1,0:T(8,128)(2,1)S(1)} %pad_maximum_fusion), channel_id=1, source_target_pairs={{0,6},{2,4},{4,2},{6,0},{8,14},{10,12},{12,10},{14,8},{16,22},{18,... | collective-permute-start | bytes 1376264 | tf_op jit(solution)/shard_map/ppermute | solution.py:52
  40.7 19.3 %collective-permute-start.8 = (bf16[4,224,256]{2,1,0:T(8,128)(2,1)S(1)}, bf16[4,224,256]{2,1,0:T(8,128)(2,1)}, u32[]{:S(2)}, u32[]{:S(2)}) collective-permute-start(bf16[4,224,256]{2,1,0:T(8,128)(2,1)S(1)} %pad_maximum_fusion), channel_id=1, source_target_pairs={{0,2},{2,0},{4,6},{6,4},{8,10},{10,8},{12,14},{14,12},{16,18},{18,... | collective-permute-start | bytes 1376264 | tf_op jit(solution)/shard_map/ppermute | solution.py:52
  40.7 21.3 %collective-permute-start.9 = (bf16[4,224,256]{2,1,0:T(8,128)(2,1)S(1)}, bf16[4,224,256]{2,1,0:T(8,128)(2,1)}, u32[]{:S(2)}, u32[]{:S(2)}) collective-permute-start(bf16[4,224,256]{2,1,0:T(8,128)(2,1)S(1)} %pad_maximum_fusion), channel_id=1, source_target_pairs={{0,4},{2,6},{4,0},{6,2},{8,12},{10,14},{12,8},{14,10},{16,20},{18,... | collective-permute-start | bytes 1376264 | tf_op jit(solution)/shard_map/ppermute | solution.py:52
  41.3 2.9 %collective-permute-start.5 = (bf16[224,256]{1,0:T(8,128)(2,1)}, bf16[224,256]{1,0:T(8,128)(2,1)S(1)}, u32[]{:S(2)}, u32[]{:S(2)}) collective-permute-start(bf16[224,256]{1,0:T(8,128)(2,1)} %collective-permute-done.4.refs_6_), channel_id=1, source_target_pairs={{1,0},{0,1},{3,2},{2,3},{5,4},{4,5},{7,6},{6,7},{9,8},{8,9},{11,10... | collective-permute-start | bytes 344072 | tf_op jit(solution)/shard_map/ppermute | solution.py:58
  42.9 1.5 %collective-permute-start.7 = (bf16[224,256]{1,0:T(8,128)(2,1)}, bf16[224,256]{1,0:T(8,128)(2,1)S(1)}, u32[]{:S(2)}, u32[]{:S(2)}) collective-permute-start(bf16[224,256]{1,0:T(8,128)(2,1)} %collective-permute-done.6.refs_8_), channel_id=1, source_target_pairs={{1,0},{0,1},{3,2},{2,3},{5,4},{4,5},{7,6},{6,7},{9,8},{8,9},{11,10... | collective-permute-start | bytes 344072 | tf_op jit(solution)/shard_map/ppermute | solution.py:58
  44.2 17.8 %copy-start.10 = (bf16[384,512]{1,0:T(8,128)(2,1)}, bf16[384,512]{1,0:T(8,128)(2,1)S(1)}, u32[]{:S(2)}) copy-start(bf16[384,512]{1,0:T(8,128)(2,1)S(1)} %multiply_convert_fusion) | copy-start | bytes 1179652
  63.4 2.8 %collective-permute-start.16 = (bf16[384,1024]{1,0:T(8,128)(2,1)}, bf16[384,1024]{1,0:T(8,128)(2,1)}, u32[]{:S(2)}, u32[]{:S(2)}) collective-permute-start(bf16[384,1024]{1,0:T(8,128)(2,1)} %convolution_convert_fusion.1), channel_id=1, source_target_pairs={{1,0},{0,1},{3,2},{2,3},{5,4},{4,5},{7,6},{6,7},{9,8},{8,9},{11,10... | collective-permute-start | bytes 2359304 | tf_op jit(solution)/shard_map/ppermute | solution.py:541
  64.0 3.8 %collective-permute-start.13 = (bf16[4,224,256]{2,1,0:T(8,128)(2,1)}, bf16[4,224,256]{2,1,0:T(8,128)(2,1)S(1)}, u32[]{:S(2)}, u32[]{:S(2)}) collective-permute-start(bf16[4,224,256]{2,1,0:T(8,128)(2,1)} %collective-permute-done.8.refs_4_), channel_id=1, source_target_pairs={{1,0},{0,1},{3,2},{2,3},{5,4},{4,5},{7,6},{6,7},{9,8},{8,9},{11,10... | collective-permute-start | bytes 1376264 | tf_op jit(solution)/shard_map/ppermute | solution.py:58
  64.1 3.7 %collective-permute-start.14 = (bf16[4,224,256]{2,1,0:T(8,128)(2,1)}, bf16[4,224,256]{2,1,0:T(8,128)(2,1)S(1)}, u32[]{:S(2)}, u32[]{:S(2)}) collective-permute-start(bf16[4,224,256]{2,1,0:T(8,128)(2,1)} %collective-permute-done.9.refs_6_), channel_id=1, source_target_pairs={{1,0},{0,1},{3,2},{2,3},{5,4},{4,5},{7,6},{6,7},{9,8},{8,9},{11,10... | collective-permute-start | bytes 1376264 | tf_op jit(solution)/shard_map/ppermute | solution.py:58
  64.6 3.4 %collective-permute-start.15 = (bf16[4,224,256]{2,1,0:T(8,128)(2,1)S(1)}, bf16[4,224,256]{2,1,0:T(8,128)(2,1)S(1)}, u32[]{:S(2)}, u32[]{:S(2)}) collective-permute-start(bf16[4,224,256]{2,1,0:T(8,128)(2,1)S(1)} %collective-permute-done.10.refs_8_), channel_id=1, source_target_pairs={{1,0},{0,1},{3,2},{2,3},{5,4},{4,5},{7,6},{6,7},{9,8},{8,9},{11,10... | collective-permute-start | bytes 1376264 | tf_op jit(solution)/shard_map/ppermute | solution.py:58
  67.7 24.2 %copy-start.13 = (bf16[512,2048]{1,0:T(8,128)(2,1)S(1)}, bf16[512,2048]{1,0:T(8,128)(2,1)}, u32[]{:S(2)}) copy-start(bf16[512,2048]{1,0:T(8,128)(2,1)} %param.34) | copy-start | bytes 6291460
  67.8 24.2 %copy-start.22 = (f32[512]{0:T(512)S(1)}, f32[512]{0:T(512)}, u32[]{:S(2)}) copy-start(f32[512]{0:T(512)} %param.32) | copy-start | bytes 6148
  92.6 2.4 %collective-permute-start.17 = (bf16[384,1024]{1,0:T(8,128)(2,1)S(1)}, bf16[384,1024]{1,0:T(8,128)(2,1)S(1)}, u32[]{:S(2)}, u32[]{:S(2)}) collective-permute-start(bf16[384,1024]{1,0:T(8,128)(2,1)S(1)} %convolution_convert_fusion), channel_id=1, source_target_pairs={{1,0},{0,1},{3,2},{2,3},{5,4},{4,5},{7,6},{6,7},{9,8},{8,9},{11,10... | collective-permute-start | bytes 2359304 | tf_op jit(solution)/shard_map/ppermute | solution.py:541
  93.1 1.8 %collective-permute-start.18 = (f32[1,384]{1,0:T(1,128)S(1)}, f32[1,384]{1,0:T(1,128)S(1)}, u32[]{:S(2)}, u32[]{:S(2)}) collective-permute-start(f32[1,384]{1,0:T(1,128)S(1)} %broadcast_in_dim.14), channel_id=1, source_target_pairs={{1,0},{0,1},{3,2},{2,3},{5,4},{4,5},{7,6},{6,7},{9,8},{8,9},{11,10... | collective-permute-start | bytes 4616 | tf_op jit(solution)/shard_map/ppermute | solution.py:58
  (21 other events, 57.0 us)

commit v3 on v2

--- a/solution.py
+++ b/solution.py
@@ -175,8 +175,8 @@
         (out_ref, max_ref, acc_ref), refs = refs[:3], refs[3:]
     else:
         (max_ref, acc_ref), refs = refs[:2], refs[2:]
-    lat_ref, rot_ref, qbd_ref, score_refs, weight_refs, refs = (
-        refs[0], refs[1], refs[2], refs[3:5], refs[5:7], refs[7:]
+    lat_ref, rot_ref, qbd_ref, turned_ref, score_refs, weight_refs, refs = (
+        refs[0], refs[1], refs[2], refs[3], refs[4:6], refs[6:8], refs[8:]
     )
     pairs = heads // 2
     parcels = max(1, pairs // 2)
@@ -188,6 +188,7 @@
     blocks = lat_ref.shape[0]
     bias_row = 2 * NOPE_DIM + ROT_DIM
 
+    turned_ref[...] = value_up_ref[...].T
     qbd_ref[...] = jnp.zeros_like(qbd_ref)
     for pair in range(pairs):
         qbd_ref[pair, bias_row : bias_row + 16, :] = (
@@ -248,7 +249,7 @@
 
         def expand_values(n):
             values = lax.dot_general(
-                value_up_ref[n * span : (n + 1) * span, :],
+                turned_ref[n * span : (n + 1) * span, :],
                 lat_ref[block],
                 (((1,), (1,)), ((), ())),
                 preferred_element_type=jnp.float32,
@@ -368,6 +369,7 @@
             pltpu.VMEM((blocks, keys, key_up.shape[0]), jnp.bfloat16),
             pltpu.VMEM((blocks, keys, 128), jnp.bfloat16),
             pltpu.VMEM((heads // 2, 256, 2 * tok_rows), jnp.bfloat16),
+            pltpu.VMEM(value_up.shape[::-1], jnp.bfloat16),
         ]
         + [pltpu.VMEM((keys, width), jnp.float32)] * 2
         + [pltpu.VMEM((keys, width), jnp.bfloat16)] * 2
@@ -472,7 +474,7 @@
 
     token_pieces = others(tokens, "tp")
     key_up = near_by(key_up)
-    value_up = value_up.T
+    value_up = near_by(value_up)
     scaled, row_scale, latent, own_rot, mine = front(
         jnp.full((1,), tp_index, jnp.int32),
         [near_by(tokens)] + token_pieces,

time: 97.7 us -> 97.9 us (level)
  local copies, waits for them, and re-layouts: 6.87 us -> 5.79 us
    unnamed x53 -> x56, local copies, waits for them, and re-layouts: 6.51 us -> 5.44 us
    ppermute x10, waiting for transfers between devices: 1.44 us -> 2.49 us  [others(): lax.ppermute(block, axis, [((i + d) % size, i) for i in range(size)])]
  transfers between devices with their start and end apart: 19 -> 19, of which waited for: 7 -> 8; matrix products, arithmetic and copies ran while one was open for 13% -> 13% of each run, Pallas kernels for 9% -> 9%
where the time goes in v3:
time: 97.9 us; the launch traced here: 96.3 us
  Pallas kernels  37.6 us (38%)
  starting transfers between devices  16.1 us (16%)
  waiting for transfers between devices  15.5 us (16%)
  other arithmetic  11.6 us (12%)
  matrix products  9.07 us (9%)
  local copies, waits for them, and re-layouts  5.79 us (6%)
    pallas_call x2, Pallas kernels, attention_stage(): pl.pallas_call(functools.partial(attention_kernel, first, last, counts, o...  32.3 us
    ppermute x4, waiting for transfers between devices, shift_by(): lax.ppermute(block, axis, [(i, i + distance) for i in devices if i + dist...  7.58 us
    ppermute x10, starting transfers between devices, others(): lax.ppermute(block, axis, [((i + d) % size, i) for i in range(size)])  7.13 us
    ppermute x3, waiting for transfers between devices, swap_bits(): lax.ppermute(block, axis, [(i, i ^ bits) for i in range(lax.axis_size(axi...  5.47 us
    unnamed x56, local copies, waits for them, and re-layouts  5.44 us
    ppermute x4, starting transfers between devices, shift_by(): lax.ppermute(block, axis, [(i, i + distance) for i in devices if i + dist...  5.34 us
    dot_general x4, matrix products, project(): return jnp.dot(scaled, weight, preferred_element_type=f32)  4.89 us
    max x6, other arithmetic, near_by(): return jnp.maximum(array, jnp.finfo(array.dtype).min)  3.73 us
  transfers between devices with their start and end apart: 19, of which 8 were waited for; matrix products, arithmetic and copies ran while one was open for 13% of the time, Pallas kernels for 9%

profile of v3, /device:TPU:31, one launch (start us, length us, event | category | flops | bytes accessed | tf_op | source)
XLA Modules:
  0.0 96.3 jit_solution(10037681715236585216)
XLA Ops:
  3.5 1.3 %broadcast_maximum_fusion.1.refs_0_ = bf16[384,1024]{1,0:T(8,128)(2,1)S(1)} fusion(bf16[384,1024]{1,0:T(8,128)(2,1)} %param.18), kind=kLoop, calls=%fused_computation.30 | loop fusion | flops 393216 | bytes 1572864 | tf_op jit(solution)/shard_map/max | solution.py:473
  5.1 2.0 %front.1 = (bf16[384,2048]{1,0:T(8,128)(2,1)S(1)}, f32[384,1]{1,0:T(8,128)S(1)}, bf16[384,256]{1,0:T(8,128)(2,1)S(1)}, bf16[384,128]{1,0:T(8,128)(2,1)S(1)}, bf16[224,256]{1,0:T(8,128)(2,1)S(1)}) custom-call(s32[1]{0:T(128)} %bitcast.6.index_ref, bf16[384,1024]{1,0:T(8,128)(2,1)S(1)} %broadcast_maximum_fusion.1.refs_0_, ...), custom_call_target="tpu_custom_call" | custom-call | flops 805306368 | bytes 8388608 | tf_op jit(solution)/shard_map/front/pallas_call | solution.py:127
  11.8 2.0 %fusion.14.refs_0_ = bf16[512,384]{1,0:T(8,128)(2,1)} fusion(f32[384]{0:T(512)S(1)} %get-tuple-element.51, bf16[384,2048]{1,0:T(8,128)(2,1)S(1)} %get-tuple-element.30, bf16[2048,512]{1,0:T(8,128)(2,1)S(1)} %copy-done.27), kind=kOutput, calls=%fused_computation.29 | convolution fusion | flops 805699584 | bytes 4064768 | tf_op jit(solution)/shard_map/dot_general | solution.py:502
  13.8 1.3 %collective-permute-start.1 = (bf16[32,512]{1,0:T(8,128)(2,1)S(1)}, bf16[32,512]{1,0:T(8,128)(2,1)S(1)}, u32[]{:S(2)}, u32[]{:S(2)}) collective-permute-start(bf16[32,512]{1,0:T(8,128)(2,1)S(1)} %slice.20), channel_id=1, source_target_pairs={{0,2},{2,4},{4,6},{6,8},{8,10},{10,12},{12,14},{14,16},{16,18},{18... | collective-permute-start | bytes 98312 | tf_op jit(solution)/shard_map/ppermute | solution.py:48
  15.8 2.7 %collective-permute-done.1.rim_ref = bf16[32,512]{1,0:T(8,128)(2,1)S(1)} collective-permute-done((bf16[32,512]{1,0:T(8,128)(2,1)S(1)}, bf16[32,512]{1,0:T(8,128)(2,1)S(1)}, u32[]{:S(2)}, u32[]{:S(2)}) %collective-permute-start.1) | collective-permute-done | bytes 32800 | tf_op jit(solution)/shard_map/ppermute | solution.py:48
  18.4 3.3 %conv.1 = f32[384,512]{1,0:T(8,128)S(1)} custom-call(bf16[384,512]{1,0:T(8,128)(2,1)S(1)} %fusion.5.gated_ref, bf16[32,512]{1,0:T(8,128)(2,1)S(1)} %collective-permute-done.1.rim_ref, f32[31,512]{1,0:T(8,128)S(1)} %copy-done.6), custom_call_target="tpu_custom_call" | custom-call | flops 609484800 | bytes 1179648 | tf_op jit(solution)/shard_map/conv/pallas_call | solution.py:425
  21.9 1.4 %collective-permute-start.11 = (f32[2,384]{1,0:T(2,128)S(1)}, f32[2,384]{1,0:T(2,128)S(1)}, u32[]{:S(2)}, u32[]{:S(2)}) collective-permute-start(f32[2,384]{1,0:T(2,128)S(1)} %pad_maximum_fusion.4), channel_id=1, source_target_pairs={{1,0},{0,1},{3,2},{2,3},{5,4},{4,5},{7,6},{6,7},{9,8},{8,9},{11,10... | collective-permute-start | bytes 9224 | tf_op jit(solution)/shard_map/ppermute | solution.py:58
  23.4 1.3 %collective-permute-start.2 = (bf16[224,256]{1,0:T(8,128)(2,1)S(1)}, bf16[224,256]{1,0:T(8,128)(2,1)}, u32[]{:S(2)}, u32[]{:S(2)}) collective-permute-start(bf16[224,256]{1,0:T(8,128)(2,1)S(1)} %get-tuple-element.33), channel_id=1, source_target_pairs={{0,8},{2,10},{4,12},{6,14},{8,16},{10,18},{12,20},{14,22},{16,24},... | collective-permute-start | bytes 344072 | tf_op jit(solution)/shard_map/ppermute | solution.py:48
  24.7 1.3 %collective-permute-start.4 = (bf16[224,256]{1,0:T(8,128)(2,1)S(1)}, bf16[224,256]{1,0:T(8,128)(2,1)}, u32[]{:S(2)}, u32[]{:S(2)}) collective-permute-start(bf16[224,256]{1,0:T(8,128)(2,1)S(1)} %get-tuple-element.33), channel_id=1, source_target_pairs={{0,16},{2,18},{4,20},{6,22},{8,24},{10,26},{12,28},{14,30},{1,17},... | collective-permute-start | bytes 344072 | tf_op jit(solution)/shard_map/ppermute | solution.py:48
  26.0 1.5 %collective-permute-start.6 = (bf16[224,256]{1,0:T(8,128)(2,1)S(1)}, bf16[224,256]{1,0:T(8,128)(2,1)}, u32[]{:S(2)}, u32[]{:S(2)}) collective-permute-start(bf16[224,256]{1,0:T(8,128)(2,1)S(1)} %get-tuple-element.33), channel_id=1, source_target_pairs={{0,24},{2,26},{4,28},{6,30},{1,25},{3,27},{5,29},{7,31}} | collective-permute-start | bytes 344072 | tf_op jit(solution)/shard_map/ppermute | solution.py:48
  27.6 1.3 %multiply_reduce_fusion = (f32[384]{0:T(512)S(1)}, f32[384,512]{1,0:T(8,128)}) fusion(f32[512]{0:T(512)S(1)} %copy-done.21, f32[512]{0:T(512)S(1)} %copy-done.22, f32[384]{0:T(512)S(1)} %add_rsqrt_fusion, f32[384,512]{1,0:T(8,128)S(1)} %conv.1, f32[384]{0:T(512)S(1)} %get-tuple-element.53), kind=kLoop, calls=%fused_computation.23 | loop fusion | flops 1965696 | bytes 1581568 | tf_op jit(solution)/shard_map/reduce_sum | solution.py:529
  30.1 2.6 %collective-permute-start.3 = (bf16[224,256]{1,0:T(8,128)(2,1)}, bf16[224,256]{1,0:T(8,128)(2,1)S(1)}, u32[]{:S(2)}, u32[]{:S(2)}) collective-permute-start(bf16[224,256]{1,0:T(8,128)(2,1)} %collective-permute-done.2.refs_4_), channel_id=1, source_target_pairs={{1,0},{0,1},{3,2},{2,3},{5,4},{4,5},{7,6},{6,7},{9,8},{8,9},{11,10... | collective-permute-start | bytes 344072 | tf_op jit(solution)/shard_map/ppermute | solution.py:58
  32.7 4.9 %collective-permute-done.4.refs_6_ = bf16[224,256]{1,0:T(8,128)(2,1)} collective-permute-done((bf16[224,256]{1,0:T(8,128)(2,1)S(1)}, bf16[224,256]{1,0:T(8,128)(2,1)}, u32[]{:S(2)}, u32[]{:S(2)}) %collective-permute-start.4) | collective-permute-done | bytes 114720 | tf_op jit(solution)/shard_map/ppermute | solution.py:48
  38.6 2.0 %collective-permute-start.10 = (bf16[4,224,256]{2,1,0:T(8,128)(2,1)S(1)}, bf16[4,224,256]{2,1,0:T(8,128)(2,1)S(1)}, u32[]{:S(2)}, u32[]{:S(2)}) collective-permute-start(bf16[4,224,256]{2,1,0:T(8,128)(2,1)S(1)} %pad_maximum_fusion), channel_id=1, source_target_pairs={{0,6},{2,4},{4,2},{6,0},{8,14},{10,12},{12,10},{14,8},{16,22},{18,... | collective-permute-start | bytes 1376264 | tf_op jit(solution)/shard_map/ppermute | solution.py:52
  41.3 1.6 %collective-permute-start.5 = (bf16[224,256]{1,0:T(8,128)(2,1)}, bf16[224,256]{1,0:T(8,128)(2,1)S(1)}, u32[]{:S(2)}, u32[]{:S(2)}) collective-permute-start(bf16[224,256]{1,0:T(8,128)(2,1)} %collective-permute-done.4.refs_6_), channel_id=1, source_target_pairs={{1,0},{0,1},{3,2},{2,3},{5,4},{4,5},{7,6},{6,7},{9,8},{8,9},{11,10... | collective-permute-start | bytes 344072 | tf_op jit(solution)/shard_map/ppermute | solution.py:58
  42.9 1.3 %multiply_convert_fusion = bf16[384,512]{1,0:T(8,128)(2,1)S(1)} fusion(f32[384,512]{1,0:T(8,128)} %get-tuple-element.56, f32[512]{0:T(512)S(1)} %copy-done.23, f32[384]{0:T(512)S(1)} %rsqrt_reduce_fusion.1), kind=kLoop, calls=%fused_computation.22 | loop fusion | flops 589824 | bytes 1183232 | tf_op jit(solution)/shard_map/convert_element_type | solution.py:532
  47.3 8.2 %attention_first.1 = (f32[12,256]{1,0:T(8,128)S(1)}, f32[12,80,256]{2,1,0:T(8,128)S(1)}) custom-call(s32[3]{0:T(128)S(1)} %pad_add_fusion.vis_ref, bf16[512,384]{1,0:T(8,128)(2,1)S(1)} %copy-done.7, bf16[256,384]{1,0:T(8,128)(2,1)S(1)} %bitcast.31, bf16[256,512]{1,0:T(8,128)(2,1)S(1)} %get-tuple-element.65.refs_2_, ...), custom_call_target="tpu_custom_call" | custom-call | flops 3019898880 | bytes 4194304 | tf_op jit(solution)/shard_map/attention_first/pallas_call | solution.py:389
  56.5 3.4 %collective-permute-done.8.refs_4_ = bf16[4,224,256]{2,1,0:T(8,128)(2,1)} collective-permute-done((bf16[4,224,256]{2,1,0:T(8,128)(2,1)S(1)}, bf16[4,224,256]{2,1,0:T(8,128)(2,1)}, u32[]{:S(2)}, u32[]{:S(2)}) %collective-permute-start.8) | collective-permute-done | bytes 458784 | tf_op jit(solution)/shard_map/ppermute | solution.py:52
  59.9 2.0 %collective-permute-done.9.refs_6_ = bf16[4,224,256]{2,1,0:T(8,128)(2,1)} collective-permute-done((bf16[4,224,256]{2,1,0:T(8,128)(2,1)S(1)}, bf16[4,224,256]{2,1,0:T(8,128)(2,1)}, u32[]{:S(2)}, u32[]{:S(2)}) %collective-permute-start.9) | collective-permute-done | bytes 458784 | tf_op jit(solution)/shard_map/ppermute | solution.py:52
  62.0 1.5 %convolution_convert_fusion.1 = bf16[384,1024]{1,0:T(8,128)(2,1)} fusion(bf16[384,512]{1,0:T(8,128)(2,1)S(1)} %multiply_convert_fusion, bf16[512,2048]{1,0:T(8,128)(2,1)S(1)} %copy-done, s32[]{:T(128)S(6)} %select_n.29), kind=kOutput, calls=%fused_computation.3 | convolution fusion | flops 403046400 | bytes 2228228 | tf_op jit(solution)/shard_map/dot_general | solution.py:574
  64.7 1.6 %fusion.10 = f32[384,1024]{1,0:T(8,128)S(1)} fusion(bf16[384,512]{1,0:T(8,128)(2,1)} %copy-done.11, bf16[512,2048]{1,0:T(8,128)(2,1)S(1)} %copy-done, s32[]{:T(128)S(6)} %select_n.27), kind=kOutput, calls=%fused_computation.16 | convolution fusion | flops 402653184 | bytes 3014660 | tf_op jit(solution)/shard_map/dot_general | solution.py:574
  66.3 1.5 %convert_add_fusion = f32[384,1024]{1,0:T(8,128)S(1)} fusion(f32[384,1024]{1,0:T(8,128)S(1)} %fusion.10, bf16[384,1024]{1,0:T(8,128)(2,1)} %collective-permute-done.16), kind=kLoop, calls=%fused_computation.1 | loop fusion | flops 786432 | bytes 3932160 | tf_op jit(solution)/shard_map/add | solution.py:580
  68.0 24.1 %attention_rest.1 = bf16[384,512]{1,0:T(8,128)(2,1)S(1)} custom-call(s32[12]{0:T(128)S(1)} %stack.87.vis_ref, bf16[512,384]{1,0:T(8,128)(2,1)S(1)} %copy-done.8, bf16[256,384]{1,0:T(8,128)(2,1)S(1)} %bitcast.32, bf16[256,512]{1,0:T(8,128)(2,1)S(1)} %get-tuple-element.65.refs_2_, bf16[256,512]{1,0:T(8,128)(2,1)S(1)} %get-tuple-element.64.refs_3_, ...), custom_call_target="tpu_custom_call" | custom-call | flops 9059696640 | bytes 4194304 | tf_op jit(solution)/shard_map/attention_rest/pallas_call | solution.py:389
  95.1 1.2 %add_convert_fusion = bf16[384,1024]{1,0:T(8,128)(2,1)} fusion(f32[384,1024]{1,0:T(8,128)S(1)} %convert_add_fusion, f32[384,1024]{1,0:T(8,128)S(1)} %fusion.7, bf16[384,1024]{1,0:T(8,128)(2,1)S(1)} %collective-permute-done.17, f32[384]{0:T(512)S(1)} %rsqrt_reduce_fusion), kind=kLoop, calls=%fused_computation | loop fusion | flops 1966080 | bytes 4720128 | tf_op jit(solution)/shard_map/convert_element_type | solution.py:595
  (117 shorter events, 20.7 us)
Async XLA Ops:
  0.0 62.0 %copy-start = (bf16[512,2048]{1,0:T(8,128)(2,1)S(1)}, bf16[512,2048]{1,0:T(8,128)(2,1)}, u32[]{:S(2)}) copy-start(bf16[512,2048]{1,0:T(8,128)(2,1)} %param.35) | copy-start | bytes 6291460
  0.0 5.1 %collective-permute-start = (bf16[384,1024]{1,0:T(8,128)(2,1)}, bf16[384,1024]{1,0:T(8,128)(2,1)S(1)}, u32[]{:S(2)}, u32[]{:S(2)}) collective-permute-start(bf16[384,1024]{1,0:T(8,128)(2,1)} %param.18), channel_id=1, source_target_pairs={{1,0},{0,1},{3,2},{2,3},{5,4},{4,5},{7,6},{6,7},{9,8},{8,9},{11,10... | collective-permute-start | bytes 2359304 | tf_op jit(solution)/shard_map/ppermute | solution.py:58
  13.8 4.6 %collective-permute-start.1 = (bf16[32,512]{1,0:T(8,128)(2,1)S(1)}, bf16[32,512]{1,0:T(8,128)(2,1)S(1)}, u32[]{:S(2)}, u32[]{:S(2)}) collective-permute-start(bf16[32,512]{1,0:T(8,128)(2,1)S(1)} %slice.20), channel_id=1, source_target_pairs={{0,2},{2,4},{4,6},{6,8},{8,10},{10,12},{12,14},{14,16},{16,18},{18... | collective-permute-start | bytes 98312 | tf_op jit(solution)/shard_map/ppermute | solution.py:48
  21.9 5.5 %collective-permute-start.11 = (f32[2,384]{1,0:T(2,128)S(1)}, f32[2,384]{1,0:T(2,128)S(1)}, u32[]{:S(2)}, u32[]{:S(2)}) collective-permute-start(f32[2,384]{1,0:T(2,128)S(1)} %pad_maximum_fusion.4), channel_id=1, source_target_pairs={{1,0},{0,1},{3,2},{2,3},{5,4},{4,5},{7,6},{6,7},{9,8},{8,9},{11,10... | collective-permute-start | bytes 9224 | tf_op jit(solution)/shard_map/ppermute | solution.py:58
  23.4 19.5 %copy-start.23 = (f32[512]{0:T(512)S(1)}, f32[512]{0:T(512)}, u32[]{:S(2)}) copy-start(f32[512]{0:T(512)} %param.33) | copy-start | bytes 6148
  23.4 6.7 %collective-permute-start.2 = (bf16[224,256]{1,0:T(8,128)(2,1)S(1)}, bf16[224,256]{1,0:T(8,128)(2,1)}, u32[]{:S(2)}, u32[]{:S(2)}) collective-permute-start(bf16[224,256]{1,0:T(8,128)(2,1)S(1)} %get-tuple-element.33), channel_id=1, source_target_pairs={{0,8},{2,10},{4,12},{6,14},{8,16},{10,18},{12,20},{14,22},{16,24},... | collective-permute-start | bytes 344072 | tf_op jit(solution)/shard_map/ppermute | solution.py:48
  24.7 12.8 %collective-permute-start.4 = (bf16[224,256]{1,0:T(8,128)(2,1)S(1)}, bf16[224,256]{1,0:T(8,128)(2,1)}, u32[]{:S(2)}, u32[]{:S(2)}) collective-permute-start(bf16[224,256]{1,0:T(8,128)(2,1)S(1)} %get-tuple-element.33), channel_id=1, source_target_pairs={{0,16},{2,18},{4,20},{6,22},{8,24},{10,26},{12,28},{14,30},{1,17},... | collective-permute-start | bytes 344072 | tf_op jit(solution)/shard_map/ppermute | solution.py:48
  26.0 11.5 %collective-permute-start.6 = (bf16[224,256]{1,0:T(8,128)(2,1)S(1)}, bf16[224,256]{1,0:T(8,128)(2,1)}, u32[]{:S(2)}, u32[]{:S(2)}) collective-permute-start(bf16[224,256]{1,0:T(8,128)(2,1)S(1)} %get-tuple-element.33), channel_id=1, source_target_pairs={{0,24},{2,26},{4,28},{6,30},{1,25},{3,27},{5,29},{7,31}} | collective-permute-start | bytes 344072 | tf_op jit(solution)/shard_map/ppermute | solution.py:48
  28.8 1.2 %collective-permute-start.12 = (f32[1,384]{1,0:T(1,128)S(1)}, f32[1,384]{1,0:T(1,128)S(1)}, u32[]{:S(2)}, u32[]{:S(2)}) collective-permute-start(f32[1,384]{1,0:T(1,128)S(1)} %broadcast_in_dim.13), channel_id=1, source_target_pairs={{1,0},{0,1},{3,2},{2,3},{5,4},{4,5},{7,6},{6,7},{9,8},{8,9},{11,10... | collective-permute-start | bytes 4616 | tf_op jit(solution)/shard_map/ppermute | solution.py:58
  30.1 12.8 %collective-permute-start.3 = (bf16[224,256]{1,0:T(8,128)(2,1)}, bf16[224,256]{1,0:T(8,128)(2,1)S(1)}, u32[]{:S(2)}, u32[]{:S(2)}) collective-permute-start(bf16[224,256]{1,0:T(8,128)(2,1)} %collective-permute-done.2.refs_4_), channel_id=1, source_target_pairs={{1,0},{0,1},{3,2},{2,3},{5,4},{4,5},{7,6},{6,7},{9,8},{8,9},{11,10... | collective-permute-start | bytes 344072 | tf_op jit(solution)/shard_map/ppermute | solution.py:58
  38.6 17.9 %collective-permute-start.10 = (bf16[4,224,256]{2,1,0:T(8,128)(2,1)S(1)}, bf16[4,224,256]{2,1,0:T(8,128)(2,1)S(1)}, u32[]{:S(2)}, u32[]{:S(2)}) collective-permute-start(bf16[4,224,256]{2,1,0:T(8,128)(2,1)S(1)} %pad_maximum_fusion), channel_id=1, source_target_pairs={{0,6},{2,4},{4,2},{6,0},{8,14},{10,12},{12,10},{14,8},{16,22},{18,... | collective-permute-start | bytes 1376264 | tf_op jit(solution)/shard_map/ppermute | solution.py:52
  40.7 19.3 %collective-permute-start.8 = (bf16[4,224,256]{2,1,0:T(8,128)(2,1)S(1)}, bf16[4,224,256]{2,1,0:T(8,128)(2,1)}, u32[]{:S(2)}, u32[]{:S(2)}) collective-permute-start(bf16[4,224,256]{2,1,0:T(8,128)(2,1)S(1)} %pad_maximum_fusion), channel_id=1, source_target_pairs={{0,2},{2,0},{4,6},{6,4},{8,10},{10,8},{12,14},{14,12},{16,18},{18,... | collective-permute-start | bytes 1376264 | tf_op jit(solution)/shard_map/ppermute | solution.py:52
  40.7 21.3 %collective-permute-start.9 = (bf16[4,224,256]{2,1,0:T(8,128)(2,1)S(1)}, bf16[4,224,256]{2,1,0:T(8,128)(2,1)}, u32[]{:S(2)}, u32[]{:S(2)}) collective-permute-start(bf16[4,224,256]{2,1,0:T(8,128)(2,1)S(1)} %pad_maximum_fusion), channel_id=1, source_target_pairs={{0,4},{2,6},{4,0},{6,2},{8,12},{10,14},{12,8},{14,10},{16,20},{18,... | collective-permute-start | bytes 1376264 | tf_op jit(solution)/shard_map/ppermute | solution.py:52
  41.3 2.9 %collective-permute-start.5 = (bf16[224,256]{1,0:T(8,128)(2,1)}, bf16[224,256]{1,0:T(8,128)(2,1)S(1)}, u32[]{:S(2)}, u32[]{:S(2)}) collective-permute-start(bf16[224,256]{1,0:T(8,128)(2,1)} %collective-permute-done.4.refs_6_), channel_id=1, source_target_pairs={{1,0},{0,1},{3,2},{2,3},{5,4},{4,5},{7,6},{6,7},{9,8},{8,9},{11,10... | collective-permute-start | bytes 344072 | tf_op jit(solution)/shard_map/ppermute | solution.py:58
  42.9 1.5 %collective-permute-start.7 = (bf16[224,256]{1,0:T(8,128)(2,1)}, bf16[224,256]{1,0:T(8,128)(2,1)S(1)}, u32[]{:S(2)}, u32[]{:S(2)}) collective-permute-start(bf16[224,256]{1,0:T(8,128)(2,1)} %collective-permute-done.6.refs_8_), channel_id=1, source_target_pairs={{1,0},{0,1},{3,2},{2,3},{5,4},{4,5},{7,6},{6,7},{9,8},{8,9},{11,10... | collective-permute-start | bytes 344072 | tf_op jit(solution)/shard_map/ppermute | solution.py:58
  44.2 17.8 %copy-start.11 = (bf16[384,512]{1,0:T(8,128)(2,1)}, bf16[384,512]{1,0:T(8,128)(2,1)S(1)}, u32[]{:S(2)}) copy-start(bf16[384,512]{1,0:T(8,128)(2,1)S(1)} %multiply_convert_fusion) | copy-start | bytes 1179652
  63.4 2.8 %collective-permute-start.16 = (bf16[384,1024]{1,0:T(8,128)(2,1)}, bf16[384,1024]{1,0:T(8,128)(2,1)}, u32[]{:S(2)}, u32[]{:S(2)}) collective-permute-start(bf16[384,1024]{1,0:T(8,128)(2,1)} %convolution_convert_fusion.1), channel_id=1, source_target_pairs={{1,0},{0,1},{3,2},{2,3},{5,4},{4,5},{7,6},{6,7},{9,8},{8,9},{11,10... | collective-permute-start | bytes 2359304 | tf_op jit(solution)/shard_map/ppermute | solution.py:543
  64.0 3.8 %collective-permute-start.13 = (bf16[4,224,256]{2,1,0:T(8,128)(2,1)}, bf16[4,224,256]{2,1,0:T(8,128)(2,1)S(1)}, u32[]{:S(2)}, u32[]{:S(2)}) collective-permute-start(bf16[4,224,256]{2,1,0:T(8,128)(2,1)} %collective-permute-done.8.refs_4_), channel_id=1, source_target_pairs={{1,0},{0,1},{3,2},{2,3},{5,4},{4,5},{7,6},{6,7},{9,8},{8,9},{11,10... | collective-permute-start | bytes 1376264 | tf_op jit(solution)/shard_map/ppermute | solution.py:58
  64.1 3.7 %collective-permute-start.14 = (bf16[4,224,256]{2,1,0:T(8,128)(2,1)}, bf16[4,224,256]{2,1,0:T(8,128)(2,1)S(1)}, u32[]{:S(2)}, u32[]{:S(2)}) collective-permute-start(bf16[4,224,256]{2,1,0:T(8,128)(2,1)} %collective-permute-done.9.refs_6_), channel_id=1, source_target_pairs={{1,0},{0,1},{3,2},{2,3},{5,4},{4,5},{7,6},{6,7},{9,8},{8,9},{11,10... | collective-permute-start | bytes 1376264 | tf_op jit(solution)/shard_map/ppermute | solution.py:58
  64.6 3.4 %collective-permute-start.15 = (bf16[4,224,256]{2,1,0:T(8,128)(2,1)S(1)}, bf16[4,224,256]{2,1,0:T(8,128)(2,1)S(1)}, u32[]{:S(2)}, u32[]{:S(2)}) collective-permute-start(bf16[4,224,256]{2,1,0:T(8,128)(2,1)S(1)} %collective-permute-done.10.refs_8_), channel_id=1, source_target_pairs={{1,0},{0,1},{3,2},{2,3},{5,4},{4,5},{7,6},{6,7},{9,8},{8,9},{11,10... | collective-permute-start | bytes 1376264 | tf_op jit(solution)/shard_map/ppermute | solution.py:58
  67.7 24.4 %copy-start.14 = (bf16[512,2048]{1,0:T(8,128)(2,1)S(1)}, bf16[512,2048]{1,0:T(8,128)(2,1)}, u32[]{:S(2)}) copy-start(bf16[512,2048]{1,0:T(8,128)(2,1)} %param.34) | copy-start | bytes 6291460
  67.8 24.4 %copy-start.24 = (f32[512]{0:T(512)S(1)}, f32[512]{0:T(512)}, u32[]{:S(2)}) copy-start(f32[512]{0:T(512)} %param.32) | copy-start | bytes 6148
  92.7 2.4 %collective-permute-start.17 = (bf16[384,1024]{1,0:T(8,128)(2,1)S(1)}, bf16[384,1024]{1,0:T(8,128)(2,1)S(1)}, u32[]{:S(2)}, u32[]{:S(2)}) collective-permute-start(bf16[384,1024]{1,0:T(8,128)(2,1)S(1)} %convolution_convert_fusion), channel_id=1, source_target_pairs={{1,0},{0,1},{3,2},{2,3},{5,4},{4,5},{7,6},{6,7},{9,8},{8,9},{11,10... | collective-permute-start | bytes 2359304 | tf_op jit(solution)/shard_map/ppermute | solution.py:543
  93.3 1.8 %collective-permute-start.18 = (f32[1,384]{1,0:T(1,128)S(1)}, f32[1,384]{1,0:T(1,128)S(1)}, u32[]{:S(2)}, u32[]{:S(2)}) collective-permute-start(f32[1,384]{1,0:T(1,128)S(1)} %broadcast_in_dim.14), channel_id=1, source_target_pairs={{1,0},{0,1},{3,2},{2,3},{5,4},{4,5},{7,6},{6,7},{9,8},{8,9},{11,10... | collective-permute-start | bytes 4616 | tf_op jit(solution)/shard_map/ppermute | solution.py:58
  (23 other events, 79.6 us)
